TPU v7x, 512 devices: a whole 4x8x8 slice. The times are simulated.
512 devices in a mesh: sp: 64 (over z, y), tp: 8 (over x, core).
Axes of the slice: x: 4, y: 8, z: 8, core: 2. Of those that a mesh axis runs over, the one named last changes fastest.
Arguments:
- resid: bfloat16 [32768, 2048], P('sp'), may hold values from -6 to 6
- queries: bfloat16 [32768, 2048], P('sp', 'tp'), may hold values from -6 to 6
- keys: bfloat16 [32768, 512], P('sp', 'tp'), may hold values from -6 to 6
- values: bfloat16 [32768, 512], P('sp', 'tp'), may hold values from -6 to 6
- documents: int32 [32768], P('sp'), may hold values from 0 to 31, never falling along the last dimension, each value on 1 to 2048 neighbouring positions
- q_gain: float32 [64], replicated, may hold values from 0.5 to 6.5
- k_gain: float32 [64], replicated, may hold values from 0.5 to 6.5
- sink: float32 [32], P('tp'), may hold values from -1 to 5
- w_out: bfloat16 [2048, 2048], P('tp'), may hold values from -0.5 to 0.5
- n_gain: float32 [2048], replicated, may hold values from 0.1 to 1.9
- w_up: bfloat16 [2048, 8192], P('sp', 'tp'), may hold values from -0.125 to 0.125
- w_down: bfloat16 [8192, 2048], P('tp', 'sp'), may hold values from -0.0625 to 0.0625
Outputs:
- layer_out: bfloat16 [32768, 2048], P('sp')
All inputs are finite; a program needn't handle non-finite values.
Results may differ from a plain program's by a relative error of at most 0.018.
The roundings to bfloat16 on the way count: a program that leaves them out, or rounds other values in their place, can miss the bound.
Values may be sent and summed in bfloat16 or wider, within the bound.
A program may use at most 64 MiB of HBM per device.

v0:
```python
import jax
import jax.numpy as jnp
from jax import lax
from jax.sharding import PartitionSpec as P

WINDOW = 128


EPS = 1e-06


def gather_turned(arrays, axis, dims):
    turned = [jnp.moveaxis(a, dim, 0) for a, dim in zip(arrays, dims)]
    both = jnp.concatenate([t.reshape(len(t), -1) for t in turned], axis=1)
    result, at, outs = (lax.all_gather(both, axis, axis=0, tiled=True), 0, [])
    for t, dim in zip(turned, dims):
        section = result[:, at : at + t[0].size].reshape(-1, *t.shape[1:])
        outs.append(jnp.moveaxis(section, 0, dim))
        at += t[0].size
    return tuple(outs)


def extended(x, sides, width):
    for axis, dim in sides:
        count, length = (lax.axis_size(axis), x.shape[dim])
        up = [(i, (i + 1) % count) for i in range(count - 1)]
        down = [(j, i) for i, j in up]
        last = lax.slice_in_dim(x, length - width, length, axis=dim)
        initial = lax.slice_in_dim(x, 0, width, axis=dim)
        before = lax.ppermute(last, axis, up)
        after = lax.ppermute(initial, axis, down)
        x = jnp.concatenate([before, x, after], axis=dim)
    return x


def in_blocks(x, dim, count):
    dims = x.shape
    tiles = x.reshape(*dims[:dim], count, dims[dim] // count, *dims[dim + 1 :])
    return jnp.moveaxis(tiles, dim, 0)


def summed_on_arrival(x, axis, dim):
    count = lax.axis_size(axis)
    tiles = lax.all_to_all(in_blocks(x, dim, count), axis, 0, 0, tiled=True)
    return jnp.sum(tiles.astype(jnp.float32), axis=0)


def joined_along(tiles, dim):
    dims = list(tiles.shape[1:])
    dims[dim] *= tiles.shape[0]
    return jnp.moveaxis(tiles, 0, dim).reshape(dims)


def copy_for_each(x, axis):
    copies = jnp.broadcast_to(x, (lax.axis_size(axis), *x.shape))
    return lax.all_to_all(copies, axis, split_axis=0, concat_axis=0, tiled=True)


def collect(x, axis, dim):
    return joined_along(copy_for_each(x, axis), dim)


def rms_scale(field, gain):
    wide = field.astype(jnp.float32)
    return wide * lax.rsqrt(jnp.mean(wide * wide, axis=-1, keepdims=True) + EPS) * gain


def mixer_partial(normed, gathered):
    upward = jnp.dot(normed, gathered[0], preferred_element_type=jnp.float32)
    active = jnp.square(jax.nn.relu(upward)).astype(jnp.bfloat16)
    return jnp.dot(active, gathered[1], preferred_element_type=jnp.float32)


def shards(
    resid, queries, keys, values, documents, q_gain, k_gain, sink, w_out, n_gain, w_up, w_down
):
    rows = resid.shape[0]
    head_size = q_gain.shape[0]
    heads_here = sink.shape[0]
    kv_here = keys.shape[1] // head_size
    group = heads_here // kv_here
    gathered = None
    gathered = gather_turned((w_up, w_down), "sp", (0, 1))
    qnorm = rms_scale(queries.reshape(rows, kv_here, group, head_size), q_gain).astype(jnp.bfloat16)
    knorm = rms_scale(keys.reshape(rows, kv_here, head_size), k_gain).astype(jnp.bfloat16)
    vheads = values.reshape(rows, kv_here, head_size)
    doc_here = documents.astype(jnp.bfloat16)
    near_keys, near_values, near_docs = (
        extended(knorm, (("sp", 0),), WINDOW),
        extended(vheads, (("sp", 0),), WINDOW),
        extended(doc_here, (("sp", 0),), WINDOW),
    )
    offset = lax.axis_index("sp") * rows
    total = rows * lax.axis_size("sp")
    query_pos = offset + jnp.arange(rows, dtype=jnp.int32)
    key_pos = offset - WINDOW + jnp.arange(rows + 2 * WINDOW, dtype=jnp.int32)
    distance = key_pos[None, :] - query_pos[:, None]
    allowed = (jnp.abs(distance) <= WINDOW) & (key_pos[None, :] >= 0) & (key_pos[None, :] < total)
    allowed = allowed & (near_docs[None, :] == doc_here[:, None])
    heads_all = heads_here * lax.axis_size("tp")
    first_head = (lax.axis_index("tp") * heads_here).astype(jnp.float32)
    slopes = jnp.exp2(
        -8.0 * (first_head + jnp.arange(heads_here, dtype=jnp.float32) + 1.0) / heads_all
    )
    slopes = slopes.reshape(kv_here, group)
    sink_f = sink.reshape(kv_here, group)
    scores = jnp.einsum(
        "rkgd,skd->kgrs", qnorm, near_keys, preferred_element_type=jnp.float32
    ) * head_size ** (-0.5)
    scores = scores - slopes[:, :, None, None] * jnp.abs(distance).astype(jnp.float32)[None, None]
    scores = jnp.where(allowed[None, None], scores, jnp.float32(-1e30))
    highest = jnp.maximum(jnp.max(scores, axis=-1), sink_f[:, :, None])
    weights = jnp.exp(scores - highest[..., None])
    denom = jnp.sum(weights, axis=-1) + jnp.exp(sink_f[:, :, None] - highest)
    summed = jnp.einsum(
        "kgrs,skd->rkgd",
        weights.astype(jnp.bfloat16),
        near_values,
        preferred_element_type=jnp.float32,
    )
    attended = (
        (summed / denom.transpose(2, 0, 1)[..., None])
        .astype(jnp.bfloat16)
        .reshape(rows, heads_here * head_size)
    )
    share = rows // lax.axis_size("tp")
    head_mix = summed_on_arrival(
        jnp.dot(attended, w_out, preferred_element_type=jnp.float32).astype(jnp.bfloat16), "tp", 0
    )
    own_resid = lax.dynamic_slice_in_dim(resid, lax.axis_index("tp") * share, share, 0)
    middle = (own_resid.astype(jnp.float32) + head_mix).astype(jnp.bfloat16)
    normed_part = rms_scale(middle, n_gain).astype(jnp.bfloat16)
    normed = collect(normed_part, "tp", 0)
    partial_sum = mixer_partial(normed, gathered)
    unit_mix = summed_on_arrival(partial_sum.astype(jnp.bfloat16), "tp", 0)
    finished = (middle.astype(jnp.float32) + unit_mix).astype(jnp.bfloat16)
    return collect(finished, "tp", 0)


def solution(mesh):
    placed = (
        P("sp", None),
        P("sp", "tp"),
        P("sp", "tp"),
        P("sp", "tp"),
        P("sp"),
        P(),
        P(),
        P("tp"),
        P("tp", None),
        P(),
        P("sp", "tp"),
        P("tp", "sp"),
    )
    return jax.shard_map(
        shards, mesh=mesh, in_specs=placed, out_specs=P("sp", None), check_vma=False
    )
```

profile of v0, /device:TPU:1, one launch (start us, length us, event | category | flops | bytes accessed | tf_op | source)
XLA Modules:
  0.0 194.1 jit_solution(1907560911907022125)
XLA Ops:
  6.5 1.6 pad_maximum_fusion
  8.9 4.0 %collective-permute-start.2 = (bf16[128]{0:T(256)(128)(2,1)S(1)}, bf16[128]{0:T(256)(128)(2,1)S(1)}, u32[]{:S(2)}, u32[]{:S(2)}) collective-permute-start(bf16[128]{0:T(256)(128)(2,1)S(1)} %get-tuple-element.11), channel_id=1, source_target_pairs={{0,8},{8,16},{16,24},{24,32},{32,40},{40,48},{48,56},{56,64},{64,7... | collective-permute-start | bytes 776 | tf_op jit(solution)/shard_map/ppermute | solution.py:30
  12.9 1.3 collective-permute-start.3
  15.1 0.9 fusion.41
  16.0 4.0 %collective-permute-start.4 = (bf16[128,1,64]{0,2,1:T(8,128)(2,1)S(1)}, bf16[128,1,64]{0,2,1:T(8,128)(2,1)S(1)}, u32[]{:S(2)}, u32[]{:S(2)}) collective-permute-start(bf16[128,1,64]{0,2,1:T(8,128)(2,1)S(1)} %get-tuple-element.9), channel_id=1, source_target_pairs={{0,8},{8,16},{16,24},{24,32},{32,40},{40,48},{48,56},{56,64},{64,7... | collective-permute-start | bytes 49160 | tf_op jit(solution)/shard_map/ppermute | solution.py:30
  20.0 1.3 collective-permute-start.5
  22.1 4.0 %collective-permute-start = (bf16[128,1,64]{0,2,1:T(8,128)(2,1)S(1)}, bf16[128,1,64]{0,2,1:T(8,128)(2,1)S(1)}, u32[]{:S(2)}, u32[]{:S(2)}) collective-permute-start(bf16[128,1,64]{0,2,1:T(8,128)(2,1)S(1)} %get-tuple-element.7), channel_id=1, source_target_pairs={{0,8},{8,16},{16,24},{24,32},{32,40},{40,48},{48,56},{56,64},{64,7... | collective-permute-start | bytes 49160 | tf_op jit(solution)/shard_map/ppermute | solution.py:30
  26.1 1.1 copy.15
  27.3 0.9 fusion.67
  29.4 1.3 collective-permute-start.1
  30.8 1.0 fusion.20
  31.8 1.9 fusion.7
  33.8 1.9 fusion.1
  35.8 2.3 %fusion.30 = bf16[512,1,4,64]{0,3,2,1:T(8,128)(2,1)S(1)} fusion(f32[768,512,4]{1,0,2:T(8,128)S(1)} %get-tuple-element.14, f32[4,512]{1,0:T(4,128)S(1)} %broadcast_maximum_fusion, f32[512,768]{0,1:T(8,128)S(1)} %fusion.16, f32[4]{0:T(128)S(1)} %multiply_exponential_fusion, pred[512,768]{0,1:T(8,128)(4,1)S(1)} %fusion.20, f32[512,4]{0,1:T(4,128)S(1)} %fusion.54, ...), kind=kOutput, calls=%fused_computation.26 | convolution fusion | flops 211320832 | bytes 8634384 | tf_op jit(solution)/shard_map/kgrs,skd->rkgd/dot_general | solution.py:115
  38.1 2.1 %convolution_convert_fusion = bf16[512,2048]{1,0:T(8,128)(2,1)} fusion(bf16[512,256]{0,1:T(8,128)(2,1)S(1)} %bitcast.93, bf16[256,2048]{1,0:T(8,128)(2,1)S(1)} %copy-done), kind=kOutput, calls=%fused_computation.15 | convolution fusion | flops 537919488 | bytes 3407872 | tf_op jit(solution)/shard_map/dot_general | solution.py:128
  40.2 8.9 %all-to-all-start = ((bf16[8,64,2048]{2,1,0:T(8,128)(2,1)}), bf16[8,64,2048]{2,1,0:T(8,128)(2,1)S(1)}, u32[]{:S(2)}, u32[]{:S(2)}) async-start(bf16[8,64,2048]{2,1,0:T(8,128)(2,1)} %bitcast.23), calls=%async_computation | async-start | bytes 4194304 | tf_op jit(solution)/shard_map/all_to_all | solution.py:44
  49.0 26.2 %all-to-all-done = bf16[8,64,2048]{2,1,0:T(8,128)(2,1)S(1)} async-done(((bf16[8,64,2048]{2,1,0:T(8,128)(2,1)}), bf16[8,64,2048]{2,1,0:T(8,128)(2,1)S(1)}, u32[]{:S(2)}, u32[]{:S(2)}) %all-to-all-start) | async-done | bytes 2097184 | tf_op jit(solution)/shard_map/all_to_all | solution.py:44
  75.6 1.1 fusion.35
  77.2 29.6 %all_to_all.20 = bf16[8,64,2048]{2,1,0:T(8,128)(2,1)S(1)} all-to-all(bf16[8,64,2048]{2,1,0:T(8,128)(2,1)S(1)} %broadcast_in_dim.14), channel_id=1, replica_groups=mesh['sp'=64,'tp'=8] {'tp'}, dimensions={0} | all-to-all | bytes 4194304 | tf_op jit(solution)/shard_map/all_to_all | solution.py:56
  106.8 8.1 %all-gather.2.cloned.1.call-done = bf16[2048,2048]{1,0:T(8,128)(2,1)} async-done(((bf16[32,2048]{1,0:T(8,128)(2,1)}), bf16[2048,2048]{1,0:T(8,128)(2,1)}) %all-gather.2.cloned.1.call-update) | async-done | bytes 8388624 | tf_op jit(solution)/shard_map/all_gather | solution.py:15
  115.0 9.3 %fusion.11 = bf16[512,2048]{1,0:T(8,128)(2,1)} fusion(bf16[2048,2048]{1,0:T(8,128)(2,1)} %all-gather.2.cloned.1.call-done, bf16[512,2048]{1,0:T(8,128)(2,1)S(1)} %bitcast.91), kind=kOutput, calls=%fused_computation.14 | convolution fusion | flops 4297588736 | bytes 12582912 | tf_op jit(solution)/shard_map/dot_general | solution.py:71
  124.3 31.3 %all_to_all.21 = bf16[8,64,2048]{2,1,0:T(8,128)(2,1)S(1)} all-to-all(bf16[8,64,2048]{2,1,0:T(8,128)(2,1)} %bitcast.92), channel_id=1, replica_groups=mesh['sp'=64,'tp'=8] {'tp'}, dimensions={0} | all-to-all | bytes 4194304 | tf_op jit(solution)/shard_map/all_to_all | solution.py:44
  156.3 29.7 %all_to_all.22 = bf16[8,64,2048]{2,1,0:T(8,128)(2,1)S(1)} all-to-all(bf16[8,64,2048]{2,1,0:T(8,128)(2,1)S(1)} %broadcast_in_dim.15), channel_id=1, replica_groups=mesh['sp'=64,'tp'=8] {'tp'}, dimensions={0} | all-to-all | bytes 4194304 | tf_op jit(solution)/shard_map/all_to_all | solution.py:56
  186.0 1.3 copy.19
  (42 shorter events, 5.2 us)
Async XLA Ops:
  6.5 31.6 %copy-start = (bf16[256,2048]{1,0:T(8,128)(2,1)S(1)}, bf16[256,2048]{1,0:T(8,128)(2,1)}, u32[]{:S(2)}) copy-start(bf16[256,2048]{1,0:T(8,128)(2,1)} %param.20) | copy-start | bytes 3145732
  6.5 108.4 %all-gather.2.cloned.1.call-start = ((), (), s32[]{:S(2)}) async-start(), calls=%async_computation.4 | async-start | bytes 8519680 | tf_op jit(solution)/shard_map/all_gather | solution.py:15
  8.9 20.5 %collective-permute-start.2 = (bf16[128]{0:T(256)(128)(2,1)S(1)}, bf16[128]{0:T(256)(128)(2,1)S(1)}, u32[]{:S(2)}, u32[]{:S(2)}) collective-permute-start(bf16[128]{0:T(256)(128)(2,1)S(1)} %get-tuple-element.11), channel_id=1, source_target_pairs={{0,8},{8,16},{16,24},{24,32},{32,40},{40,48},{48,56},{56,64},{64,7... | collective-permute-start | bytes 776 | tf_op jit(solution)/shard_map/ppermute | solution.py:30
  12.9 17.8 %collective-permute-start.3 = (bf16[128]{0:T(256)(128)(2,1)S(1)}, bf16[128]{0:T(256)(128)(2,1)S(1)}, u32[]{:S(2)}, u32[]{:S(2)}) collective-permute-start(bf16[128]{0:T(256)(128)(2,1)S(1)} %get-tuple-element.12), channel_id=1, source_target_pairs={{8,0},{16,8},{24,16},{32,24},{40,32},{48,40},{56,48},{64,56},{72,6... | collective-permute-start | bytes 776 | tf_op jit(solution)/shard_map/ppermute | solution.py:31
  16.0 15.7 %collective-permute-start.4 = (bf16[128,1,64]{0,2,1:T(8,128)(2,1)S(1)}, bf16[128,1,64]{0,2,1:T(8,128)(2,1)S(1)}, u32[]{:S(2)}, u32[]{:S(2)}) collective-permute-start(bf16[128,1,64]{0,2,1:T(8,128)(2,1)S(1)} %get-tuple-element.9), channel_id=1, source_target_pairs={{0,8},{8,16},{16,24},{24,32},{32,40},{40,48},{48,56},{56,64},{64,7... | collective-permute-start | bytes 49160 | tf_op jit(solution)/shard_map/ppermute | solution.py:30
  20.0 11.8 %collective-permute-start.5 = (bf16[128,1,64]{0,2,1:T(8,128)(2,1)S(1)}, bf16[128,1,64]{0,2,1:T(8,128)(2,1)S(1)}, u32[]{:S(2)}, u32[]{:S(2)}) collective-permute-start(bf16[128,1,64]{0,2,1:T(8,128)(2,1)S(1)} %get-tuple-element.10), channel_id=1, source_target_pairs={{8,0},{16,8},{24,16},{32,24},{40,32},{48,40},{56,48},{64,56},{72,6... | collective-permute-start | bytes 49160 | tf_op jit(solution)/shard_map/ppermute | solution.py:31
  22.1 13.7 %collective-permute-start = (bf16[128,1,64]{0,2,1:T(8,128)(2,1)S(1)}, bf16[128,1,64]{0,2,1:T(8,128)(2,1)S(1)}, u32[]{:S(2)}, u32[]{:S(2)}) collective-permute-start(bf16[128,1,64]{0,2,1:T(8,128)(2,1)S(1)} %get-tuple-element.7), channel_id=1, source_target_pairs={{0,8},{8,16},{16,24},{24,32},{32,40},{40,48},{48,56},{56,64},{64,7... | collective-permute-start | bytes 49160 | tf_op jit(solution)/shard_map/ppermute | solution.py:30
  29.4 6.3 %collective-permute-start.1 = (bf16[128,1,64]{0,2,1:T(8,128)(2,1)S(1)}, bf16[128,1,64]{0,2,1:T(8,128)(2,1)S(1)}, u32[]{:S(2)}, u32[]{:S(2)}) collective-permute-start(bf16[128,1,64]{0,2,1:T(8,128)(2,1)S(1)} %get-tuple-element.8), channel_id=1, source_target_pairs={{8,0},{16,8},{24,16},{32,24},{40,32},{48,40},{56,48},{64,56},{72,6... | collective-permute-start | bytes 49160 | tf_op jit(solution)/shard_map/ppermute | solution.py:31
  31.8 1.9 copy-start.3
  33.7 2.1 %copy-start.1 = (bf16[512,64]{0,1:T(8,128)(2,1)S(1)}, bf16[512,64]{0,1:T(8,128)(2,1)}, u32[]{:S(2)}) copy-start(bf16[512,64]{0,1:T(8,128)(2,1)} %param.15) | copy-start | bytes 196612
  40.2 36.6 %copy-start.2 = (f32[2048]{0:T(1024)S(1)}, f32[2048]{0:T(1024)}, u32[]{:S(2)}) copy-start(f32[2048]{0:T(1024)} %param.21) | copy-start | bytes 24580
  40.2 35.1 %all-to-all-start = ((bf16[8,64,2048]{2,1,0:T(8,128)(2,1)}), bf16[8,64,2048]{2,1,0:T(8,128)(2,1)S(1)}, u32[]{:S(2)}, u32[]{:S(2)}) async-start(bf16[8,64,2048]{2,1,0:T(8,128)(2,1)} %bitcast.23), calls=%async_computation | async-start | bytes 4194304 | tf_op jit(solution)/shard_map/all_to_all | solution.py:44
Sparse Core Ops, SparseCore 0:
  10.4 104.5 all-gather.1
where the time goes:
time: 195 us; the launch traced here: 194 us
  blocking collectives  90.6 us (46%)
  waiting for transfers between devices  34.4 us (18%)
  starting transfers between devices  24.7 us (13%)
  matrix products  15.6 us (8%)
  between operations  13.7 us (7%)
  other arithmetic  10.7 us (5%)
  local copies, waits for them, and re-layouts  4.41 us (2%)
    all_to_all x2, blocking collectives, copy_for_each(): return lax.all_to_all(copies, axis, split_axis=0, concat_axis=0, tiled=True)  59.3 us
    all_to_all x1, blocking collectives, summed_on_arrival(): tiles = lax.all_to_all(in_blocks(x, dim, count), axis, 0, 0, tiled=True)  31.3 us
    all_to_all x1, waiting for transfers between devices, summed_on_arrival(): tiles = lax.all_to_all(in_blocks(x, dim, count), axis, 0, 0, tiled=True)  26.2 us
    ppermute x3, starting transfers between devices, extended(): before = lax.ppermute(last, axis, up)  12 us
    dot_general x1, matrix products, mixer_partial(): return jnp.dot(active, gathered[1], preferred_element_type=jnp.float32)  9.31 us
    all_to_all x1, starting transfers between devices, summed_on_arrival(): tiles = lax.all_to_all(in_blocks(x, dim, count), axis, 0, 0, tiled=True)  8.88 us
    all_gather x1, waiting for transfers between devices, gather_turned(): result, at, outs = (lax.all_gather(both, axis, axis=0, tiled=True), 0, [])  8.14 us
  transfers between devices with their start and end apart: 8, of which 2 were waited for; matrix products, arithmetic and copies ran while one was open for 9% of the time, Pallas kernels for 0%

commit v1 on v0

v1 whole, which is shorter than its diff:
```python
import functools

import jax
import jax.numpy as jnp
from jax import lax
from jax.experimental import pallas as pl
from jax.experimental.pallas import tpu as pltpu
from jax.sharding import PartitionSpec as P

WINDOW = 128
EPS = 1e-06
Z, Y, X, C = 8, 8, 4, 2
MESH = pl.DeviceIdType.MESH
BF, F32 = jnp.bfloat16, jnp.float32
NC1, NC2 = 2, 4


def extended(x, sides, width):
    for axis, dim in sides:
        count, length = (lax.axis_size(axis), x.shape[dim])
        up = [(i, (i + 1) % count) for i in range(count - 1)]
        down = [(j, i) for i, j in up]
        last = lax.slice_in_dim(x, length - width, length, axis=dim)
        initial = lax.slice_in_dim(x, 0, width, axis=dim)
        before = lax.ppermute(last, axis, up)
        after = lax.ppermute(initial, axis, down)
        x = jnp.concatenate([before, x, after], axis=dim)
    return x


def rms_scale(field, gain):
    wide = field.astype(F32)
    return wide * lax.rsqrt(jnp.mean(wide * wide, axis=-1, keepdims=True) + EPS) * gain


def fused(
    att, wout_h, resid_h, gain, wup_h, wdt_h, out,
    WU, WD, WO, RES, PB1, RB1, SND1, RCV1, PB2, RB2, SND2, RCV2, NALL, MID, ACC, ACT,
    loc, g1s, g1r, g2s, g2r, d1s, d1r, n1s, n1r, d2s, d2r, n2s, n2r, a1s, a1r, a2s, a2r,
):
    sp, tp = lax.axis_index("sp"), lax.axis_index("tp")
    z, y = sp // Y, sp % Y
    x, c = tp // C, tp % C
    co = 1 - c

    def at_z(s):
        return (((z + s + Z) % Z) * Y + y, tp)

    def at_y(s):
        return (z * Y + (y + s + Y) % Y, tp)

    def xm(s):
        return (x + s + X) % X

    def at_x(s):
        return (sp, xm(s) * C + c)

    partner = (sp, x * C + co)
    pending = []

    def rc(src, dst, ss, rs, dev):
        return pltpu.make_async_remote_copy(
            src_ref=src, dst_ref=dst, send_sem=ss, recv_sem=rs, device_id=dev, device_id_type=MESH
        )

    def put(src, dst, ss, rs, dev):
        rc(src, dst, ss, rs, dev).start()
        pending.append(lambda: rc(src, dst, ss, rs, dev).wait_send())

    def got(ref, ss, rs):
        rc(ref, ref, ss, rs, partner).wait_recv()

    loads = [
        pltpu.make_async_copy(wup_h, WU.at[y, z], loc.at[0]),
        pltpu.make_async_copy(wdt_h, WD.at[z, y], loc.at[1]),
        pltpu.make_async_copy(wout_h, WO, loc.at[2]),
        pltpu.make_async_copy(
            resid_h.at[pl.ds(pl.multiple_of(tp * 64, 64), 64)], RES, loc.at[3]
        ),
    ]
    for copy in loads:
        copy.start()
    barrier = pltpu.get_barrier_semaphore()
    near = [at_z(1), at_z(-1), at_y(1), at_y(-1), at_x(1), at_x(-1), partner]
    for dev in near:
        pl.semaphore_signal(barrier, inc=1, device_id=dev, device_id_type=MESH)
    loads[0].wait()
    loads[1].wait()
    pl.semaphore_wait(barrier, len(near))

    streams = []
    for w, (buf, ma, mi, dma, dmi) in enumerate(
        ((WU, y, z, at_y, at_z), (WD, z, y, at_z, at_y))
    ):
        for e, s in enumerate((1, -1)):
            streams.append((2 * w + e, buf, ma, mi, dma(s), dmi(s), s, e))

    def minor_off(j):
        return jnp.where(j % 2 == 1, -((j + 1) // 2), j // 2)

    def first_ref(st, d, at_me):
        i, buf, ma, mi, _, _, s, e = st
        dist = d if at_me else d - 1
        ref = buf.at[ma, (mi - s * dist + 8) % 8]
        return ref.at[pl.ds(16 * e, 16)] if d == 4 else ref

    def first_send(st, d):
        i, buf, ma, mi, _, dev, s, e = st
        src = first_ref(st, d, False)
        put(src, src, g1s.at[i, d - 1], g1r.at[i, d - 1], dev)

    def first_got(st, d):
        i = st[0]
        got(first_ref(st, d, True), g1s.at[i, d - 1], g1r.at[i, d - 1])

    def second_copy(st, d, j, m):
        i, buf, ma, mi, dev, _, s, e = st
        src = buf.at[(ma - s * (d - 1) + 8) % 8, (mi + minor_off(j) + 8) % 8]
        return rc(src, src, g2s.at[i, m], g2r.at[i, m], dev)

    def second_got(st, d, j, m):
        i, buf, ma, mi, dev, _, s, e = st
        ref = buf.at[(ma - s * d + 16) % 8, (mi + minor_off(j) + 8) % 8]
        got(ref, g2s.at[i, m], g2r.at[i, m])

    def second_first(j):
        for st in streams:
            second_copy(st, 1, j, j).start()

    def pump(lo, hi):
        def both(m, _):
            d, j = m // 8 + 1, m % 8
            for st in streams:
                second_got(st, d, j, m)
                second_copy(st, d + 1, j, m + 8).start()
            return 0

        def half(m, _, es):
            d, j = m // 8 + 1, m % 8
            for st in streams:
                second_got(st, d, j, m)
                if st[7] in es:
                    second_copy(st, 4, j, m + 8 - 4 * st[7]).start()
            return 0

        def last(m, _):
            for st in streams:
                second_got(st, 4, m - 24 + 4 * st[7], m)
            return 0

        for a, b, f in (
            (0, 16, both),
            (16, 20, functools.partial(half, es=(0,))),
            (20, 24, functools.partial(half, es=(1,))),
            (24, 28, last),
        ):
            a, b = max(a, lo), min(b, hi)
            if a < b:
                lax.fori_loop(a, b, f, 0)

    def minor_step(d):
        for st in streams:
            first_got(st, d)
        if d < 4:
            for st in streams:
                first_send(st, d + 1)
            second_first(2 * d - 1)
            second_first(2 * d)
        else:
            second_first(7)

    class Exchange:
        def __init__(self, PB, RB, SND, RCV, ds, dr, ns, nr):
            self.PB, self.RB, self.SND, self.RCV = PB, RB, SND, RCV
            self.ds, self.dr, self.ns, self.nr = ds, dr, ns, nr

        def to_partner(self, k):
            for q in (2, 1, 3, 0):
                b = xm(q)
                put(self.PB.at[k, b * C + co], self.RB.at[k, b], self.ds.at[k, q],
                    self.dr.at[k, q], partner)

        def pair(self, k, q, side):
            b = xm(q)
            return self.PB[k, b * C + c, side].astype(F32) + self.RB[k, b, side].astype(F32)

        def partner_got(self, k, q):
            got(self.RB.at[k, xm(q)], self.ds.at[k, q], self.dr.at[k, q])

        def send(self, k, slot, value, dirn):
            self.SND[k, slot] = value.astype(BF)
            put(self.SND.at[k, slot], self.RCV.at[k, slot], self.ns.at[k, slot],
                self.nr.at[k, slot], at_x(dirn))

        def have(self, k, slot):
            got(self.RCV.at[k, slot], self.ns.at[k, slot], self.nr.at[k, slot])
            return self.RCV[k, slot].astype(F32)

        def far(self, k):
            self.partner_got(k, 2)
            self.send(k, 0, self.pair(k, 2, 0), 1)
            self.send(k, 1, self.pair(k, 2, 1), -1)
            self.partner_got(k, 1)
            self.send(k, 2, self.pair(k, 1, 1), 1)
            self.partner_got(k, 3)
            self.send(k, 3, self.pair(k, 3, 0), -1)

        def grow(self, k):
            self.send(k, 4, self.pair(k, 1, 0) + self.have(k, 0), 1)
            self.send(k, 5, self.pair(k, 3, 1) + self.have(k, 1), -1)

        def total(self, k):
            self.partner_got(k, 0)
            left = self.pair(k, 0, 0) + self.have(k, 3) + self.have(k, 4)
            right = self.pair(k, 0, 1) + self.have(k, 2) + self.have(k, 5)
            return left, right

    class Gather:
        def __init__(self, G, cols, s, r):
            self.G, self.cols, self.s, self.r = G, cols, s, r

        def ref(self, k, q, side, core):
            return self.G.at[xm(q) * C + core, :, self.cols(k, side)]

        def go(self, k, slot, q, side, dev):
            ref = self.ref(k, q, side, c)
            put(ref, ref, self.s.at[k, slot], self.r.at[k, slot], dev)

        def wait(self, k, slot, q, side, core):
            got(self.ref(k, q, side, core), self.s.at[k, slot], self.r.at[k, slot])

        def own(self, k):
            self.go(k, 0, 0, 0, at_x(1))
            self.go(k, 1, 0, 1, at_x(-1))
            self.go(k, 2, 0, 1, at_x(1))
            self.go(k, 3, 0, 0, at_x(-1))
            self.go(k, 6, 0, 0, partner)
            self.go(k, 7, 0, 1, partner)

        def forward(self, k):
            self.wait(k, 0, 3, 0, c)
            self.go(k, 4, 3, 0, at_x(1))
            self.wait(k, 1, 1, 1, c)
            self.go(k, 5, 1, 1, at_x(-1))
            self.go(k, 8, 3, 0, partner)
            self.go(k, 9, 1, 1, partner)

        def forward2(self, k):
            self.wait(k, 2, 3, 1, c)
            self.go(k, 10, 3, 1, partner)
            self.wait(k, 3, 1, 0, c)
            self.go(k, 11, 1, 0, partner)

        def last(self, k):
            self.wait(k, 4, 2, 0, c)
            self.go(k, 12, 2, 0, partner)
            self.wait(k, 5, 2, 1, c)
            self.go(k, 13, 2, 1, partner)

        def finish(self, k):
            for slot, q, side in (
                (6, 0, 0), (7, 0, 1), (8, 3, 0), (9, 1, 1), (10, 3, 1), (11, 1, 0),
                (12, 2, 0), (13, 2, 1),
            ):
                self.wait(k, slot, q, side, co)

    one = Exchange(PB1, RB1, SND1, RCV1, d1s, d1r, n1s, n1r)
    two = Exchange(PB2, RB2, SND2, RCV2, d2s, d2r, n2s, n2r)
    rows = Gather(NALL, lambda k, side: pl.ds(side * 1024, 1024), a1s, a1r)
    pairs = ((0, -1), (1, -2), (2, -3), (3, -4))

    def block_of(k, side):
        return (z + pairs[k][side] + 8) % 8

    def out_cols(k, side):
        return pl.ds(pl.multiple_of(block_of(k, side) * 256, 256), 256)

    done = Gather(out, out_cols, a2s, a2r)

    for st in streams:
        first_send(st, 1)
    second_first(0)

    loads[2].wait()
    a = att[...]
    H1 = 2048 // (2 * NC1)
    for k in range(NC1):
        for side in range(2):
            lo = (2 * k + side) * H1
            p = jnp.dot(a, WO[:, lo:lo + H1], preferred_element_type=F32).astype(BF)
            PB1[k, :, side] = p.reshape(8, 64, H1)
        one.to_partner(k)
    minor_step(1)
    for k in range(NC1):
        one.far(k)
    minor_step(2)
    for k in range(NC1):
        one.grow(k)
    minor_step(3)
    minor_step(4)
    loads[3].wait()
    pump(0, 4)
    for k in range(NC1):
        for side, part in enumerate(one.total(k)):
            lo = (2 * k + side) * H1
            MID[:, lo:lo + H1] = (RES[:, lo:lo + H1].astype(F32) + part).astype(BF).astype(F32)
    mid = MID[...]
    scale = lax.rsqrt(jnp.mean(mid * mid, axis=-1, keepdims=True) + EPS)
    normed = (mid * scale * gain[...]).astype(BF).astype(F32)
    lane = lax.broadcasted_iota(jnp.int32, (64, 128), 1) // 32
    own = NALL.at[x * C + c]
    for yy in range(8):
        for h in range(2):
            got_cols = None
            for q in range(4):
                lo = (4 * h + q) * 256 + (yy // 4) * 128
                piece = normed[:, lo:lo + 128]
                shift = ((q - yy % 4) * 32) % 128
                if shift:
                    piece = pltpu.roll(piece, shift, axis=1)
                got_cols = piece if got_cols is None else jnp.where(lane == q, piece, got_cols)
            own[:, yy * 256 + h * 128:yy * 256 + h * 128 + 128] = got_cols.astype(BF)
    rows.own(0)
    pump(4, 8)
    rows.forward(0)
    rows.forward2(0)
    pump(8, 12)
    rows.last(0)
    rows.finish(0)

    def up_block(off, first):
        q = (y + off + 8) % 8

        def tile(n, _):
            lhs = NALL[:, :, pl.ds(pl.multiple_of(q * 256, 256), 256)].reshape(512, 256)
            rhs = WU[q, :, :, pl.ds(pl.multiple_of(n * 256, 256), 256)].reshape(256, 256)
            d = jnp.dot(lhs, rhs, preferred_element_type=F32)
            if first:
                ACC[n] = d
            else:
                ACC[n] += d
            return 0

        lax.fori_loop(0, 4, tile, 0)

    up_block(0, True)
    up_block(-1, False)
    up_block(1, False)
    pump(12, 16)
    up_block(-2, False)
    up_block(2, False)
    pump(16, 24)
    up_block(-3, False)
    up_block(3, False)
    pump(24, 28)
    up_block(4, False)

    def squared(n, _):
        r = jnp.maximum(ACC[n], 0.0)
        ACT[:, pl.ds(pl.multiple_of(n * 256, 256), 256)] = (r * r).astype(BF)
        return 0

    lax.fori_loop(0, 4, squared, 0)

    def s_down(k):
        for side in range(2):
            w = WD[block_of(k, side)].reshape(256, 1024)
            p = lax.dot_general(
                ACT[...], w, (((1,), (1,)), ((), ())), preferred_element_type=F32
            ).astype(BF)
            PB2[k, :, side] = p.reshape(8, 64, 256)
        two.to_partner(k)

    def s_total(k):
        for side, part in enumerate(two.total(k)):
            cols = out_cols(k, side)
            out[x * C + c, :, cols] = (MID[:, cols] + part).astype(BF)
        done.own(k)

    stages = (
        s_down, two.far, two.grow, s_total, done.forward, done.forward2, done.last, done.finish
    )
    for t in range(NC2 + len(stages) - 1):
        for i, stage in enumerate(stages):
            if 0 <= t - i < NC2:
                stage(t - i)

    for wait in pending:
        wait()

    def sent(m, _):
        for st in streams:
            ref = st[1].at[0, 0]
            rc(ref, ref, g2s.at[st[0], m], g2r.at[st[0], m], st[4]).wait_send()
        return 0

    lax.fori_loop(0, 28, sent, 0)


def layer(att, w_out, resid, n_gain, w_up, wdt):
    rows, width = resid.shape
    vm, hbm = pl.BlockSpec(memory_space=pltpu.VMEM), pl.BlockSpec(memory_space=pl.ANY)
    H1, H2 = 2048 // (2 * NC1), 2048 // (2 * NC2)
    dma = pltpu.SemaphoreType.DMA
    out = pl.pallas_call(
        fused,
        out_shape=jax.ShapeDtypeStruct((8, rows // 8, width), BF),
        in_specs=[vm, hbm, hbm, vm, hbm, hbm],
        out_specs=vm,
        scratch_shapes=[
            pltpu.VMEM((8, 8, 32, 1024), BF),
            pltpu.VMEM((8, 8, 32, 1024), BF),
            pltpu.VMEM((256, 2048), BF),
            pltpu.VMEM((64, 2048), BF),
            pltpu.VMEM((NC1, 8, 2, 64, H1), BF),
            pltpu.VMEM((NC1, 4, 2, 64, H1), BF),
            pltpu.VMEM((NC1, 6, 64, H1), BF),
            pltpu.VMEM((NC1, 6, 64, H1), BF),
            pltpu.VMEM((NC2, 8, 2, 64, H2), BF),
            pltpu.VMEM((NC2, 4, 2, 64, H2), BF),
            pltpu.VMEM((NC2, 6, 64, H2), BF),
            pltpu.VMEM((NC2, 6, 64, H2), BF),
            pltpu.VMEM((8, 64, 2048), BF),
            pltpu.VMEM((64, 2048), F32),
            pltpu.VMEM((4, 512, 256), F32),
            pltpu.VMEM((512, 1024), BF),
            dma((4,)),
            dma((4, 4)), dma((4, 4)),
            dma((4, 28)), dma((4, 28)),
            dma((NC1, 4)), dma((NC1, 4)), dma((NC1, 6)), dma((NC1, 6)),
            dma((NC2, 4)), dma((NC2, 4)), dma((NC2, 6)), dma((NC2, 6)),
            dma((1, 14)), dma((1, 14)), dma((NC2, 14)), dma((NC2, 14)),
        ],
        compiler_params=pltpu.CompilerParams(
            collective_id=0, has_side_effects=True, vmem_limit_bytes=60 * 1024 * 1024
        ),
        name="layer",
    )(att, w_out, resid, n_gain.reshape(1, -1), w_up, wdt)
    return out.reshape(rows, width)


def shards(
    resid, queries, keys, values, documents, q_gain, k_gain, sink, w_out, n_gain, w_up, w_down
):
    rows = resid.shape[0]
    head_size = q_gain.shape[0]
    heads_here = sink.shape[0]
    kv_here = keys.shape[1] // head_size
    group = heads_here // kv_here
    qnorm = rms_scale(queries.reshape(rows, kv_here, group, head_size), q_gain).astype(BF)
    knorm = rms_scale(keys.reshape(rows, kv_here, head_size), k_gain).astype(BF)
    vheads = values.reshape(rows, kv_here, head_size)
    doc_here = documents.astype(BF)
    near_keys, near_values, near_docs = (
        extended(knorm, (("sp", 0),), WINDOW),
        extended(vheads, (("sp", 0),), WINDOW),
        extended(doc_here, (("sp", 0),), WINDOW),
    )
    offset = lax.axis_index("sp") * rows
    total = rows * lax.axis_size("sp")
    query_pos = offset + jnp.arange(rows, dtype=jnp.int32)
    key_pos = offset - WINDOW + jnp.arange(rows + 2 * WINDOW, dtype=jnp.int32)
    distance = key_pos[None, :] - query_pos[:, None]
    allowed = (jnp.abs(distance) <= WINDOW) & (key_pos[None, :] >= 0) & (key_pos[None, :] < total)
    allowed = allowed & (near_docs[None, :] == doc_here[:, None])
    heads_all = heads_here * lax.axis_size("tp")
    first_head = (lax.axis_index("tp") * heads_here).astype(F32)
    slopes = jnp.exp2(-8.0 * (first_head + jnp.arange(heads_here, dtype=F32) + 1.0) / heads_all)
    slopes = slopes.reshape(kv_here, group)
    sink_f = sink.reshape(kv_here, group)
    scores = jnp.einsum(
        "rkgd,skd->kgrs", qnorm, near_keys, preferred_element_type=F32
    ) * head_size ** (-0.5)
    scores = scores - slopes[:, :, None, None] * jnp.abs(distance).astype(F32)[None, None]
    scores = jnp.where(allowed[None, None], scores, F32(-1e30))
    highest = jnp.maximum(jnp.max(scores, axis=-1), sink_f[:, :, None])
    weights = jnp.exp(scores - highest[..., None])
    denom = jnp.sum(weights, axis=-1) + jnp.exp(sink_f[:, :, None] - highest)
    summed = jnp.einsum(
        "kgrs,skd->rkgd", weights.astype(BF), near_values, preferred_element_type=F32
    )
    attended = (
        (summed / denom.transpose(2, 0, 1)[..., None])
        .astype(BF)
        .reshape(rows, heads_here * head_size)
    )
    return layer(attended, w_out, resid, n_gain, w_up, w_down.T)


def solution(mesh):
    placed = (
        P("sp", None), P("sp", "tp"), P("sp", "tp"), P("sp", "tp"), P("sp"), P(), P(),
        P("tp"), P("tp", None), P(), P("sp", "tp"), P("tp", "sp"),
    )
    return jax.shard_map(
        shards, mesh=mesh, in_specs=placed, out_specs=P("sp", None), check_vma=False
    )
```

time: 195 us -> 134 us (0.69)
  Pallas kernels: 0 us -> 99.9 us
  blocking collectives: 90.6 us -> 0 us
  waiting for transfers between devices: 34.4 us -> 0.02 us
  between operations: 13.7 us -> 0.24 us
  matrix products: 15.6 us -> 4.2 us
  starting transfers between devices: 24.7 us -> 15.8 us
  other arithmetic: 10.7 us -> 7.01 us
  local copies, waits for them, and re-layouts: 4.41 us -> 6.61 us
    pallas_call x0 -> x1, Pallas kernels: none -> 99.9 us  [layer(): pl.pallas_call(fused, out_shape=jax.ShapeDtypeStruct((8, rows // 8, width...]
    all_to_all x3 -> x0, blocking collectives: 90.6 us -> none  [the longest x2 59.3 us: copy_for_each(): return lax.all_to_all(copies, axis, split_axis=0, concat_axis=0, tiled=True)]
    all_to_all x1 -> x0, waiting for transfers between devices: 26.2 us -> none  [summed_on_arrival(): tiles = lax.all_to_all(in_blocks(x, dim, count), axis, 0, 0, tiled=True)]
    dot_general x4 -> x2, matrix products: 15.6 us -> 4.2 us  [the longest x1 2.35 us: shards(): jnp.einsum('kgrs,skd->rkgd', weights.astype(BF), near_values, preferred_e...]
    all_to_all x1 -> x0, starting transfers between devices: 8.88 us -> none  [summed_on_arrival(): tiles = lax.all_to_all(in_blocks(x, dim, count), axis, 0, 0, tiled=True)]
    all_gather x1 -> x0, waiting for transfers between devices: 8.14 us -> none  [gather_turned(): result, at, outs = (lax.all_gather(both, axis, axis=0, tiled=True), 0, [])]
    unnamed x10 -> x6, local copies, waits for them, and re-layouts: 2.43 us -> 4.26 us
  transfers between devices with their start and end apart: 8 -> 6, of which waited for: 2 -> 0; matrix products, arithmetic and copies ran while one was open for 9% -> 8% of each run, Pallas kernels for 0% -> 0%
where the time goes in v1:
time: 134 us
  Pallas kernels  99.9 us (75%)
  starting transfers between devices  15.8 us (12%)
  other arithmetic  7.01 us (5%)
  local copies, waits for them, and re-layouts  6.61 us (5%)
  matrix products  4.2 us (3%)
    pallas_call x1, Pallas kernels, layer(): pl.pallas_call(fused, out_shape=jax.ShapeDtypeStruct((8, rows // 8, width...  99.9 us
    ppermute x3, starting transfers between devices, extended(): before = lax.ppermute(last, axis, up)  12 us
    unnamed x6, local copies, waits for them, and re-layouts  4.26 us
    ppermute x3, starting transfers between devices, extended(): after = lax.ppermute(initial, axis, down)  3.88 us
  transfers between devices with their start and end apart: 6, of which 0 were waited for; matrix products, arithmetic and copies ran while one was open for 8% of the time, Pallas kernels for 0%

profile of v1, /device:TPU:1, one launch (start us, length us, event | category | flops | bytes accessed | tf_op | source)
XLA Modules:
  0.0 133.9 jit_solution(8124406657101924530)
XLA Ops:
  0.0 0.7 convert_element_type.53
  0.7 4.0 %collective-permute-start.2 = (bf16[128]{0:T(256)(128)(2,1)S(1)}, bf16[128]{0:T(256)(128)(2,1)S(1)}, u32[]{:S(2)}, u32[]{:S(2)}) collective-permute-start(bf16[128]{0:T(256)(128)(2,1)S(1)} %get-tuple-element.9), channel_id=1, source_target_pairs={{0,8},{8,16},{16,24},{24,32},{32,40},{40,48},{48,56},{56,64},{64,7... | collective-permute-start | bytes 776 | tf_op jit(solution)/shard_map/ppermute | solution.py:25
  4.7 1.3 collective-permute-start.3
  6.0 0.9 fusion.23
  6.9 0.9 fusion.25
  7.8 4.0 %collective-permute-start.4 = (bf16[128,1,64]{0,2,1:T(8,128)(2,1)S(1)}, bf16[128,1,64]{0,2,1:T(8,128)(2,1)S(1)}, u32[]{:S(2)}, u32[]{:S(2)}) collective-permute-start(bf16[128,1,64]{0,2,1:T(8,128)(2,1)S(1)} %get-tuple-element.7), channel_id=1, source_target_pairs={{0,8},{8,16},{16,24},{24,32},{32,40},{40,48},{48,56},{56,64},{64,7... | collective-permute-start | bytes 49160 | tf_op jit(solution)/shard_map/ppermute | solution.py:25
  11.8 1.3 collective-permute-start.5
  13.1 0.7 slice_bitcast_fusion.3
  13.9 4.0 %collective-permute-start = (bf16[128,1,64]{0,2,1:T(8,128)(2,1)S(1)}, bf16[128,1,64]{0,2,1:T(8,128)(2,1)S(1)}, u32[]{:S(2)}, u32[]{:S(2)}) collective-permute-start(bf16[128,1,64]{0,2,1:T(8,128)(2,1)S(1)} %get-tuple-element.5), channel_id=1, source_target_pairs={{0,8},{8,16},{16,24},{24,32},{32,40},{40,48},{48,56},{56,64},{64,7... | collective-permute-start | bytes 49160 | tf_op jit(solution)/shard_map/ppermute | solution.py:25
  17.9 0.9 fusion.47
  18.8 1.1 copy.16
  20.0 0.3 fusion.7
  20.4 0.7 mul.118
  21.1 0.1 mul.119
  21.1 0.1 fusion.22
  21.3 1.3 collective-permute-start.1
  22.6 1.0 fusion.11
  23.6 1.9 %fusion.3 = (f32[4,512]{1,0:T(4,128)S(1)}, f32[768,512,4]{1,0,2:T(8,128)S(1)}) fusion(f32[512,768]{0,1:T(8,128)S(1)} %fusion.7, f32[4]{0:T(128)S(1)} %multiply_exponential_fusion, pred[512,768]{0,1:T(8,128)(4,1)S(1)} %fusion.11, bf16[512,4,64]{0,2,1:T(8,128)(2,1)S(1)} %bitcast.86, bf16[128,1,64]{0,2,1:T(8,128)(2,1)S(1)} %collective-permute-done.5, ...), kind=kOutput, calls=%fused_computation.5 | convolution fusion | flops 209483776 | bytes 8626192 | tf_op jit(solution)/shard_map/rkgd,skd->kgrs/dot_general | solution.py:471
  25.6 1.9 %fusion.1 = f32[4,512]{1,0:T(4,128)S(1)} fusion(f32[768,512,4]{1,0,2:T(8,128)S(1)} %get-tuple-element.12, f32[4,512]{1,0:T(4,128)S(1)} %broadcast_maximum_fusion, f32[512,768]{0,1:T(8,128)S(1)} %fusion.7, f32[4]{0:T(128)S(1)} %multiply_exponential_fusion, pred[512,768]{0,1:T(8,128)(4,1)S(1)} %fusion.11), kind=kLoop, calls=%fused_computation.3 | loop fusion | flops 9435136 | bytes 8273936 | tf_op jit(solution)/shard_map/reduce_sum | solution.py:478
  27.5 0.1 fusion.38
  27.6 2.4 %fusion.18 = bf16[512,1,4,64]{0,3,2,1:T(8,128)(2,1)S(1)} fusion(f32[768,512,4]{1,0,2:T(8,128)S(1)} %get-tuple-element.12, f32[4,512]{1,0:T(4,128)S(1)} %broadcast_maximum_fusion, f32[512,768]{0,1:T(8,128)S(1)} %fusion.7, f32[4]{0:T(128)S(1)} %multiply_exponential_fusion, pred[512,768]{0,1:T(8,128)(4,1)S(1)} %fusion.11, f32[512,4]{0,1:T(4,128)S(1)} %fusion.38, ...), kind=kOutput, calls=%fused_computation.16 | convolution fusion | flops 211320832 | bytes 8634384 | tf_op jit(solution)/shard_map/kgrs,skd->rkgd/dot_general | solution.py:479
  29.9 0.8 copy.18.att
  30.8 99.9 %layer.1 = bf16[8,64,2048]{2,1,0:T(8,128)(2,1)} custom-call(bf16[512,256]{1,0:T(8,128)(2,1)} %copy.18.att, bf16[256,2048]{1,0:T(8,128)(2,1)} %wout_h.1, bf16[512,2048]{1,0:T(8,128)(2,1)} %resid_h.1, f32[1,2048]{1,0:T(1,128)} %bitcast.90, bf16[32,1024]{1,0:T(8,128)(2,1)} %wup_h.1, bf16[32,1024]{1,0:T(8,128)(2,1)} %bitcast.88), custom_call_target="tpu_custom_call" | custom-call | tf_op jit(solution)/shard_map/layer/pallas_call | solution.py:405
  130.7 3.2 %copy.21 = bf16[512,2048]{1,0:T(8,128)(2,1)} copy(bf16[512,2048]{1,0:T(8,128)(2,1)} %bitcast.85) | data formatting | bytes 4194304
  (21 shorter events, 0.2 us)
Async XLA Ops:
  0.7 20.6 %collective-permute-start.2 = (bf16[128]{0:T(256)(128)(2,1)S(1)}, bf16[128]{0:T(256)(128)(2,1)S(1)}, u32[]{:S(2)}, u32[]{:S(2)}) collective-permute-start(bf16[128]{0:T(256)(128)(2,1)S(1)} %get-tuple-element.9), channel_id=1, source_target_pairs={{0,8},{8,16},{16,24},{24,32},{32,40},{40,48},{48,56},{56,64},{64,7... | collective-permute-start | bytes 776 | tf_op jit(solution)/shard_map/ppermute | solution.py:25
  4.7 17.9 %collective-permute-start.3 = (bf16[128]{0:T(256)(128)(2,1)S(1)}, bf16[128]{0:T(256)(128)(2,1)S(1)}, u32[]{:S(2)}, u32[]{:S(2)}) collective-permute-start(bf16[128]{0:T(256)(128)(2,1)S(1)} %get-tuple-element.10), channel_id=1, source_target_pairs={{8,0},{16,8},{24,16},{32,24},{40,32},{48,40},{56,48},{64,56},{72,6... | collective-permute-start | bytes 776 | tf_op jit(solution)/shard_map/ppermute | solution.py:26
  7.8 15.8 %collective-permute-start.4 = (bf16[128,1,64]{0,2,1:T(8,128)(2,1)S(1)}, bf16[128,1,64]{0,2,1:T(8,128)(2,1)S(1)}, u32[]{:S(2)}, u32[]{:S(2)}) collective-permute-start(bf16[128,1,64]{0,2,1:T(8,128)(2,1)S(1)} %get-tuple-element.7), channel_id=1, source_target_pairs={{0,8},{8,16},{16,24},{24,32},{32,40},{40,48},{48,56},{56,64},{64,7... | collective-permute-start | bytes 49160 | tf_op jit(solution)/shard_map/ppermute | solution.py:25
  11.8 11.8 %collective-permute-start.5 = (bf16[128,1,64]{0,2,1:T(8,128)(2,1)S(1)}, bf16[128,1,64]{0,2,1:T(8,128)(2,1)S(1)}, u32[]{:S(2)}, u32[]{:S(2)}) collective-permute-start(bf16[128,1,64]{0,2,1:T(8,128)(2,1)S(1)} %get-tuple-element.8), channel_id=1, source_target_pairs={{8,0},{16,8},{24,16},{32,24},{40,32},{48,40},{56,48},{64,56},{72,6... | collective-permute-start | bytes 49160 | tf_op jit(solution)/shard_map/ppermute | solution.py:26
  13.9 13.7 %collective-permute-start = (bf16[128,1,64]{0,2,1:T(8,128)(2,1)S(1)}, bf16[128,1,64]{0,2,1:T(8,128)(2,1)S(1)}, u32[]{:S(2)}, u32[]{:S(2)}) collective-permute-start(bf16[128,1,64]{0,2,1:T(8,128)(2,1)S(1)} %get-tuple-element.5), channel_id=1, source_target_pairs={{0,8},{8,16},{16,24},{24,32},{32,40},{40,48},{48,56},{56,64},{64,7... | collective-permute-start | bytes 49160 | tf_op jit(solution)/shard_map/ppermute | solution.py:25
  20.0 5.4 %copy-start.1 = (f32[4]{0:T(128)S(1)}, f32[4]{0:T(128)}, u32[]{:S(2)}) copy-start(f32[4]{0:T(128)} %param.19) | copy-start | bytes 52
  21.3 6.3 %collective-permute-start.1 = (bf16[128,1,64]{0,2,1:T(8,128)(2,1)S(1)}, bf16[128,1,64]{0,2,1:T(8,128)(2,1)S(1)}, u32[]{:S(2)}, u32[]{:S(2)}) collective-permute-start(bf16[128,1,64]{0,2,1:T(8,128)(2,1)S(1)} %get-tuple-element.6), channel_id=1, source_target_pairs={{8,0},{16,8},{24,16},{32,24},{40,32},{48,40},{56,48},{64,56},{72,6... | collective-permute-start | bytes 49160 | tf_op jit(solution)/shard_map/ppermute | solution.py:26
  25.5 2.1 %copy-start = (bf16[512,64]{0,1:T(8,128)(2,1)S(1)}, bf16[512,64]{0,1:T(8,128)(2,1)}, u32[]{:S(2)}) copy-start(bf16[512,64]{0,1:T(8,128)(2,1)} %param.15) | copy-start | bytes 196612

commit v2 on v1

--- a/solution.py
+++ b/solution.py
@@ -7,7 +7,6 @@
 from jax.experimental.pallas import tpu as pltpu
 from jax.sharding import PartitionSpec as P
 
-WINDOW = 128
 EPS = 1e-06
 Z, Y, X, C = 8, 8, 4, 2
 MESH = pl.DeviceIdType.MESH
@@ -15,28 +14,10 @@
 NC1, NC2 = 2, 4
 
 
-def extended(x, sides, width):
-    for axis, dim in sides:
-        count, length = (lax.axis_size(axis), x.shape[dim])
-        up = [(i, (i + 1) % count) for i in range(count - 1)]
-        down = [(j, i) for i, j in up]
-        last = lax.slice_in_dim(x, length - width, length, axis=dim)
-        initial = lax.slice_in_dim(x, 0, width, axis=dim)
-        before = lax.ppermute(last, axis, up)
-        after = lax.ppermute(initial, axis, down)
-        x = jnp.concatenate([before, x, after], axis=dim)
-    return x
-
-
-def rms_scale(field, gain):
-    wide = field.astype(F32)
-    return wide * lax.rsqrt(jnp.mean(wide * wide, axis=-1, keepdims=True) + EPS) * gain
-
-
 def fused(
-    att, wout_h, resid_h, gain, wup_h, wdt_h, out,
-    WU, WD, WO, RES, PB1, RB1, SND1, RCV1, PB2, RB2, SND2, RCV2, NALL, MID, ACC, ACT,
-    loc, g1s, g1r, g2s, g2r, d1s, d1r, n1s, n1r, d2s, d2r, n2s, n2r, a1s, a1r, a2s, a2r,
+    q_h, k_h, v_h, doc_h, qg, kg, sink, wout_h, resid_h, gain, wup_h, wdt_h, out,
+    QX, KX, VX, DX, KN, ATT, WU, WD, WO, RES, PB1, RB1, SND1, RCV1, PB2, RB2, SND2, RCV2, NALL, MID, ACC, ACT,
+    loc, hs, hr, g1s, g1r, g2s, g2r, d1s, d1r, n1s, n1r, d2s, d2r, n2s, n2r, a1s, a1r, a2s, a2r,
 ):
     sp, tp = lax.axis_index("sp"), lax.axis_index("tp")
     z, y = sp // Y, sp % Y
@@ -72,20 +53,25 @@
 
     loads = [
         pltpu.make_async_copy(wup_h, WU.at[y, z], loc.at[0]),
-        pltpu.make_async_copy(wdt_h, WD.at[z, y], loc.at[1]),
-        pltpu.make_async_copy(wout_h, WO, loc.at[2]),
+        pltpu.make_async_copy(k_h, KX.at[:, pl.ds(128, 512)], loc.at[1]),
+        pltpu.make_async_copy(v_h, VX.at[:, pl.ds(128, 512)], loc.at[2]),
+        pltpu.make_async_copy(doc_h, DX.at[pl.ds(1, 4)], loc.at[3]),
+        pltpu.make_async_copy(wdt_h, WD.at[z, y], loc.at[4]),
+        pltpu.make_async_copy(q_h, QX, loc.at[5]),
+        pltpu.make_async_copy(wout_h, WO, loc.at[6]),
         pltpu.make_async_copy(
-            resid_h.at[pl.ds(pl.multiple_of(tp * 64, 64), 64)], RES, loc.at[3]
+            resid_h.at[pl.ds(pl.multiple_of(tp * 64, 64), 64)], RES, loc.at[7]
         ),
     ]
     for copy in loads:
         copy.start()
     barrier = pltpu.get_barrier_semaphore()
-    near = [at_z(1), at_z(-1), at_y(1), at_y(-1), at_x(1), at_x(-1), partner]
+    after, before = ((sp + 1) % (Z * Y), tp), ((sp + Z * Y - 1) % (Z * Y), tp)
+    near = [at_z(1), at_z(-1), at_y(1), at_y(-1), at_x(1), at_x(-1), partner, after, before]
     for dev in near:
         pl.semaphore_signal(barrier, inc=1, device_id=dev, device_id_type=MESH)
-    loads[0].wait()
-    loads[1].wait()
+    for copy in loads[:5]:
+        copy.wait()
     pl.semaphore_wait(barrier, len(near))
 
     streams = []
@@ -277,12 +263,99 @@
 
     done = Gather(out, out_cols, a2s, a2r)
 
+    halo = []
+    for i, ref in enumerate((KX, VX, DX)):
+        part = [
+            ref.at[pl.ds(n, 1)] if i == 2 else ref.at[:, pl.ds(128 * n, 128)] for n in range(6)
+        ]
+        put(part[4], part[0], hs.at[0, i], hr.at[0, i], after)
+        put(part[1], part[5], hs.at[1, i], hr.at[1, i], before)
+        halo.append((part[0], part[5]))
+
+    def halo_got(side):
+        for i in range(3):
+            got(halo[i][side], hs.at[side, i], hr.at[side, i])
+
     for st in streams:
         first_send(st, 1)
     second_first(0)
 
-    loads[2].wait()
-    a = att[...]
+    def head_norm(rows_, gain_, ones):
+        wide = rows_.astype(F32)
+        square = wide * wide
+        high = square.astype(BF)
+        low = (square - high.astype(F32)).astype(BF)
+        mean = (
+            jnp.dot(high, ones, preferred_element_type=F32)
+            + jnp.dot(low, ones, preferred_element_type=F32)
+        ) * (1.0 / 64)
+        return (wide * lax.rsqrt(mean + EPS) * gain_).astype(BF)
+
+    def iotas(rows_, cols_):
+        return [lax.broadcasted_iota(jnp.int32, (rows_, cols_), i) for i in range(2)]
+
+    r64, c64 = iotas(64, 64)
+    kgain = jnp.sum(jnp.where(r64 == c64, kg[...], 0.0), axis=1, keepdims=True)
+    r256, c256 = iotas(256, 256)
+    ones256 = (r256 // 64 == c256 // 64).astype(BF)
+
+    def key_norm(lo, n):
+        wide = KX[:, lo:lo + n].astype(F32)
+        mean = jnp.mean(wide * wide, axis=0, keepdims=True)
+        KN[:, lo:lo + n] = (wide * lax.rsqrt(mean + EPS) * kgain).astype(BF)
+
+    key_norm(128, 512)
+    loads[5].wait()
+    qgain = jnp.concatenate([qg[...]] * 4, axis=1)
+    heads = [
+        jnp.exp2(jnp.full((1, 1), (tp * 4 + h + 1).astype(F32) * -0.25)) for h in range(4)
+    ]
+    row = lax.broadcasted_iota(jnp.int32, (128, 128), 0)
+    col = lax.broadcasted_iota(jnp.int32, (128, 128), 1)
+    span = jnp.abs(
+        lax.broadcasted_iota(jnp.int32, (128, 384), 1) - 128
+        - lax.broadcasted_iota(jnp.int32, (128, 384), 0)
+    ).astype(F32)
+
+    def attend(b):
+        qn = head_norm(QX[128 * b:128 * b + 128], qgain, ones256)
+        kb, vb = KN[:, 128 * b:128 * b + 384], VX[:, 128 * b:128 * b + 384]
+        docs = [DX[b + i].astype(F32) for i in range(3)]
+        mine = jnp.transpose(jnp.broadcast_to(docs[1], (128, 128)))
+        if b == 0:
+            docs[0] = jnp.where(sp == 0, -1.0, docs[0])
+        if b == 3:
+            docs[2] = jnp.where(sp == Z * Y - 1, -1.0, docs[2])
+        allowed = jnp.concatenate(
+            [(mine == docs[0]) & (col >= row), mine == docs[1], (mine == docs[2]) & (col <= row)],
+            axis=1,
+        )
+        outs = []
+        for h in range(4):
+            score = jnp.dot(qn[:, 64 * h:64 * h + 64], kb, preferred_element_type=F32)
+            score = score * 0.125 - heads[h] * span
+            score = jnp.where(allowed, score, -1e30)
+            top = jnp.maximum(jnp.max(score, axis=1, keepdims=True), sink[h])
+            p = jnp.exp(score - top)
+            denom = jnp.sum(p, axis=1, keepdims=True) + jnp.exp(sink[h] - top)
+            mixed = lax.dot_general(
+                p.astype(BF), vb, (((1,), (1,)), ((), ())), preferred_element_type=F32
+            )
+            outs.append((mixed / denom).astype(BF))
+        ATT[128 * b:128 * b + 128] = jnp.concatenate(outs, axis=1)
+
+    attend(1)
+    minor_step(1)
+    attend(2)
+    halo_got(0)
+    key_norm(0, 128)
+    attend(0)
+    minor_step(2)
+    halo_got(1)
+    key_norm(640, 128)
+    attend(3)
+    loads[6].wait()
+    a = ATT[...]
     H1 = 2048 // (2 * NC1)
     for k in range(NC1):
         for side in range(2):
@@ -290,15 +363,13 @@
             p = jnp.dot(a, WO[:, lo:lo + H1], preferred_element_type=F32).astype(BF)
             PB1[k, :, side] = p.reshape(8, 64, H1)
         one.to_partner(k)
-    minor_step(1)
+    minor_step(3)
     for k in range(NC1):
         one.far(k)
-    minor_step(2)
     for k in range(NC1):
         one.grow(k)
-    minor_step(3)
     minor_step(4)
-    loads[3].wait()
+    loads[7].wait()
     pump(0, 4)
     for k in range(NC1):
         for side, part in enumerate(one.total(k)):
@@ -397,17 +468,26 @@
     lax.fori_loop(0, 28, sent, 0)
 
 
-def layer(att, w_out, resid, n_gain, w_up, wdt):
+def shards(
+    resid, queries, keys, values, documents, q_gain, k_gain, sink, w_out, n_gain, w_up, w_down
+):
     rows, width = resid.shape
-    vm, hbm = pl.BlockSpec(memory_space=pltpu.VMEM), pl.BlockSpec(memory_space=pl.ANY)
+    vm, sm = pl.BlockSpec(memory_space=pltpu.VMEM), pl.BlockSpec(memory_space=pltpu.SMEM)
+    hbm = pl.BlockSpec(memory_space=pltpu.HBM)
     H1, H2 = 2048 // (2 * NC1), 2048 // (2 * NC2)
     dma = pltpu.SemaphoreType.DMA
     out = pl.pallas_call(
         fused,
         out_shape=jax.ShapeDtypeStruct((8, rows // 8, width), BF),
-        in_specs=[vm, hbm, hbm, vm, hbm, hbm],
+        in_specs=[hbm, hbm, hbm, hbm, vm, vm, sm, hbm, hbm, vm, hbm, hbm],
         out_specs=vm,
         scratch_shapes=[
+            pltpu.VMEM((512, 256), BF),
+            pltpu.VMEM((64, 768), BF),
+            pltpu.VMEM((64, 768), BF),
+            pltpu.VMEM((6, 1, 128), jnp.int32),
+            pltpu.VMEM((64, 768), BF),
+            pltpu.VMEM((512, 256), BF),
             pltpu.VMEM((8, 8, 32, 1024), BF),
             pltpu.VMEM((8, 8, 32, 1024), BF),
             pltpu.VMEM((256, 2048), BF),
@@ -424,7 +504,7 @@
             pltpu.VMEM((64, 2048), F32),
             pltpu.VMEM((4, 512, 256), F32),
             pltpu.VMEM((512, 1024), BF),
-            dma((4,)),
+            dma((8,)), dma((2, 3)), dma((2, 3)),
             dma((4, 4)), dma((4, 4)),
             dma((4, 28)), dma((4, 28)),
             dma((NC1, 4)), dma((NC1, 4)), dma((NC1, 6)), dma((NC1, 6)),
@@ -435,56 +515,11 @@
             collective_id=0, has_side_effects=True, vmem_limit_bytes=60 * 1024 * 1024
         ),
         name="layer",
-    )(att, w_out, resid, n_gain.reshape(1, -1), w_up, wdt)
+    )(
+        queries, keys.T, values.T, documents.reshape(4, 1, 128), q_gain.reshape(1, -1),
+        k_gain.reshape(1, -1), sink, w_out, resid, n_gain.reshape(1, -1), w_up, w_down.T,
+    )
     return out.reshape(rows, width)
-
-
-def shards(
-    resid, queries, keys, values, documents, q_gain, k_gain, sink, w_out, n_gain, w_up, w_down
-):
-    rows = resid.shape[0]
-    head_size = q_gain.shape[0]
-    heads_here = sink.shape[0]
-    kv_here = keys.shape[1] // head_size
-    group = heads_here // kv_here
-    qnorm = rms_scale(queries.reshape(rows, kv_here, group, head_size), q_gain).astype(BF)
-    knorm = rms_scale(keys.reshape(rows, kv_here, head_size), k_gain).astype(BF)
-    vheads = values.reshape(rows, kv_here, head_size)
-    doc_here = documents.astype(BF)
-    near_keys, near_values, near_docs = (
-        extended(knorm, (("sp", 0),), WINDOW),
-        extended(vheads, (("sp", 0),), WINDOW),
-        extended(doc_here, (("sp", 0),), WINDOW),
-    )
-    offset = lax.axis_index("sp") * rows
-    total = rows * lax.axis_size("sp")
-    query_pos = offset + jnp.arange(rows, dtype=jnp.int32)
-    key_pos = offset - WINDOW + jnp.arange(rows + 2 * WINDOW, dtype=jnp.int32)
-    distance = key_pos[None, :] - query_pos[:, None]
-    allowed = (jnp.abs(distance) <= WINDOW) & (key_pos[None, :] >= 0) & (key_pos[None, :] < total)
-    allowed = allowed & (near_docs[None, :] == doc_here[:, None])
-    heads_all = heads_here * lax.axis_size("tp")
-    first_head = (lax.axis_index("tp") * heads_here).astype(F32)
-    slopes = jnp.exp2(-8.0 * (first_head + jnp.arange(heads_here, dtype=F32) + 1.0) / heads_all)
-    slopes = slopes.reshape(kv_here, group)
-    sink_f = sink.reshape(kv_here, group)
-    scores = jnp.einsum(
-        "rkgd,skd->kgrs", qnorm, near_keys, preferred_element_type=F32
-    ) * head_size ** (-0.5)
-    scores = scores - slopes[:, :, None, None] * jnp.abs(distance).astype(F32)[None, None]
-    scores = jnp.where(allowed[None, None], scores, F32(-1e30))
-    highest = jnp.maximum(jnp.max(scores, axis=-1), sink_f[:, :, None])
-    weights = jnp.exp(scores - highest[..., None])
-    denom = jnp.sum(weights, axis=-1) + jnp.exp(sink_f[:, :, None] - highest)
-    summed = jnp.einsum(
-        "kgrs,skd->rkgd", weights.astype(BF), near_values, preferred_element_type=F32
-    )
-    attended = (
-        (summed / denom.transpose(2, 0, 1)[..., None])
-        .astype(BF)
-        .reshape(rows, heads_here * head_size)
-    )
-    return layer(attended, w_out, resid, n_gain, w_up, w_down.T)
 
 
 def solution(mesh):

time: 134 us -> 103 us (0.77)
  starting transfers between devices: 15.8 us -> 0 us
  other arithmetic: 7.01 us -> 0 us
  matrix products: 4.2 us -> 0 us
  local copies, waits for them, and re-layouts: 6.61 us -> 3.16 us
    ppermute x6 -> x0, starting transfers between devices: 15.8 us -> none  [the longest x3 12 us: extended(): before = lax.ppermute(last, axis, up)]
    dot_general x2 -> x0, matrix products: 4.2 us -> none  [the longest x1 2.35 us: shards(): jnp.einsum('kgrs,skd->rkgd', weights.astype(BF), near_values, preferred_e...]
    convert_element_type x5 -> x0, other arithmetic: 2.98 us -> none  [the longest x2 1.86 us: shards(): knorm = rms_scale(keys.reshape(rows, kv_here, head_size), k_gain).astype(BF)]
    reduce_sum x3 -> x0, other arithmetic: 2.84 us -> none  [the longest x1 1.89 us: shards(): denom = jnp.sum(weights, axis=-1) + jnp.exp(sink_f[:, :, None] - highest)]
    unnamed x6 -> x1, local copies, waits for them, and re-layouts: 4.26 us -> 3.16 us
  transfers between devices with their start and end apart: 6 -> 0, of which waited for: 0 -> 0; matrix products, arithmetic and copies ran while one was open for 8% -> 0% of each run, Pallas kernels for 0% -> 0%
where the time goes in v2:
time: 103 us; the launch traced here: 102 us
  Pallas kernels  99.2 us (96%)
  local copies, waits for them, and re-layouts  3.16 us (3%)
    pallas_call x1, Pallas kernels, shards(): pl.pallas_call(fused, out_shape=jax.ShapeDtypeStruct((8, rows // 8, width...  99.2 us
    unnamed x1, local copies, waits for them, and re-layouts  3.16 us

profile of v2, /device:TPU:1, one launch (start us, length us, event | category | flops | bytes accessed | tf_op | source)
XLA Modules:
  0.0 102.4 jit_solution(3606366644610585844)
XLA Ops:
  0.0 99.2 %layer.1 = bf16[8,64,2048]{2,1,0:T(8,128)(2,1)} custom-call(bf16[512,256]{1,0:T(8,128)(2,1)} %q_h.1, bf16[64,512]{1,0:T(8,128)(2,1)} %bitcast.9, bf16[64,512]{1,0:T(8,128)(2,1)} %bitcast.10, s32[4,1,128]{2,1,0:T(1,128)} %bitcast.13, f32[1,64]{1,0:T(1,128)} %bitcast.14, f32[1,64]{1,0:T(1,128)} %bitcast.15, f32[4]{0:T(128)} %sink.1, bf16[256,2048]{1,0:T(8,128)(2,1)} %wout_h.1, ...), custom_call_target="tpu_custom_call" | custom-call | tf_op jit(solution)/shard_map/layer/pallas_call | solution.py:479
  99.2 3.2 %copy.14 = bf16[512,2048]{1,0:T(8,128)(2,1)} copy(bf16[512,2048]{1,0:T(8,128)(2,1)} %bitcast.8) | data formatting | bytes 4194304

commit v3 on v2

v3 whole, which is shorter than its diff:
```python
import functools

import jax
import jax.numpy as jnp
from jax import lax
from jax.experimental import pallas as pl
from jax.experimental.pallas import tpu as pltpu
from jax.sharding import PartitionSpec as P

EPS = 1e-06
Z, Y, X, C = 8, 8, 4, 2
MESH = pl.DeviceIdType.MESH
BF, F32 = jnp.bfloat16, jnp.float32
NC1, NC2 = 2, 4


def fused(
    q_h, k_h, v_h, doc_h, qg, kg, sink, wout_h, resid_h, gain, wup_h, wdt_h, out,
    QX, KX, VX, DX, KN, ATT, WU, WD, WO, RES, PB1, RB1, SND1, RCV1, PB2, RB2, SND2, RCV2, NALL, MID, ACT, OWN,
    loc, left, hr, gr, rr, fr, er, d1r, n1r, d2r, n2r, a1r, a2r,
):
    sp, tp = lax.axis_index("sp"), lax.axis_index("tp")
    z, y = sp // Y, sp % Y
    x, c = tp // C, tp % C
    co = 1 - c

    def at_z(s):
        return (((z + s + Z) % Z) * Y + y, tp)

    def at_y(s):
        return (z * Y + (y + s + Y) % Y, tp)

    def xm(s):
        return (x + s + X) % X

    def at_x(s):
        return (sp, xm(s) * C + c)

    partner = (sp, x * C + co)

    def rc(src, dst, ss, rs, dev):
        return pltpu.make_async_remote_copy(
            src_ref=src, dst_ref=dst, send_sem=ss, recv_sem=rs, device_id=dev, device_id_type=MESH
        )

    def put(src, dst, ss, rs, dev):
        rc(src, dst, ss, rs, dev).start()

    def got(ref, rs):
        rc(ref, ref, left.at[0], rs, partner).wait_recv()

    loads = [
        pltpu.make_async_copy(wup_h, WU.at[z, y], loc.at[0]),
        pltpu.make_async_copy(k_h, KX.at[:, pl.ds(128, 512)], loc.at[1]),
        pltpu.make_async_copy(v_h, VX.at[:, pl.ds(128, 512)], loc.at[2]),
        pltpu.make_async_copy(doc_h, DX.at[pl.ds(1, 4)], loc.at[3]),
        pltpu.make_async_copy(wdt_h, WD.at[z, y], loc.at[4]),
        pltpu.make_async_copy(q_h, QX, loc.at[5]),
        pltpu.make_async_copy(wout_h, WO, loc.at[6]),
        pltpu.make_async_copy(
            resid_h.at[pl.ds(pl.multiple_of(tp * 64, 64), 64)], RES, loc.at[7]
        ),
    ]
    for copy in loads:
        copy.start()
    barrier = pltpu.get_barrier_semaphore()
    after, before = ((sp + 1) % (Z * Y), tp), ((sp + Z * Y - 1) % (Z * Y), tp)
    near = [at_z(1), at_z(-1), at_y(1), at_y(-1), at_x(1), at_x(-1), partner, after, before]
    for dev in near:
        pl.semaphore_signal(barrier, inc=1, device_id=dev, device_id_type=MESH)
    pl.semaphore_wait(barrier, len(near))

    pieces = ((WU, 0, 512, "z"), (WU, 512, 512, "y"))
    ways = ((0, 1), (1, -1))

    def shard_ref(p, e, major, minor, half):
        buf, lo, n, axis = pieces[p]
        zz, yy = ((z + minor + 16) % 8, (y + major + 16) % 8)
        if axis == "y":
            zz, yy = ((z + major + 16) % 8, (y + minor + 16) % 8)
        rows_ = pl.ds(16 * e, 16) if half else slice(None)
        return buf.at[zz, yy, rows_, pl.ds(lo, n)]

    def ring_send(p, d):
        for e, s in ways:
            src = shard_ref(p, e, 0, -s * (d - 1), d == 4)
            dev = at_z(s) if pieces[p][3] == "z" else at_y(s)
            put(src, src, left.at[0], rr.at[p, e, d - 1], dev)

    def minor_off(j):
        return jnp.where(j % 2 == 1, -((j + 1) // 2), j // 2)

    def row_copy(p, e, s, d, j, m):
        src = shard_ref(p, e, -s * (d - 1), minor_off(j), False)
        dev = at_y(s) if pieces[p][3] == "z" else at_z(s)
        return rc(src, src, left.at[1], gr.at[p, e, m], dev)

    def row_got(p, e, s, d, j, m):
        got(shard_ref(p, e, -s * d, minor_off(j), False), gr.at[p, e, m])

    def row_send(p, j):
        for e, s in ways:
            row_copy(p, e, s, 1, j, j).start()

    def ring_step(ps, d):
        for p in ps:
            for e, s in ways:
                got(shard_ref(p, e, 0, -s * d, d == 4), rr.at[p, e, d - 1])
            if d < 4:
                ring_send(p, d + 1)
        for j in (2 * d - 1, 2 * d):
            if j < 8:
                for p in ps:
                    row_send(p, j)

    def pump(ps, lo, hi):
        def on(m, _):
            d, j = m // 8 + 1, m % 8
            for p in ps:
                for e, s in ways:
                    row_got(p, e, s, d, j, m)
                    row_copy(p, e, s, d + 1, j, m + 8).start()
            return 0

        def half(m, _, to):
            for p in ps:
                for e, s in ways:
                    row_got(p, e, s, 3, m - 16, m)
                    if e == to:
                        row_copy(p, e, s, 4, m - 16, m + 8 - 4 * e).start()
            return 0

        def last(m, _):
            for p in ps:
                for e, s in ways:
                    row_got(p, e, s, 4, m - 24 + 4 * e, m)
            return 0

        for a, b, f in (
            (0, 16, on),
            (16, 20, functools.partial(half, to=0)),
            (20, 24, functools.partial(half, to=1)),
            (24, 28, last),
        ):
            a, b = max(a, lo), min(b, hi)
            if b - a == 1:
                f(a, 0)
            elif a < b:
                lax.fori_loop(a, b, f, 0)

    ring_base = (0, -3, 3, 4)

    def down_ref(e, dz, dy, half):
        ref = WD.at[(z + dz + 16) % 8, (y + dy + 16) % 8]
        return ref.at[pl.ds(16 * e, 16)] if half else ref

    def loop_send(r, d):
        for e, s in ways:
            src = down_ref(e, ring_base[r], -s * (d - 1), d == 4)
            put(src, src, left.at[2], er.at[r, e, d - 1], at_y(s))

    def loop_step(r, d):
        for e, s in ways:
            got(down_ref(e, ring_base[r], -s * d, d == 4), er.at[r, e, d - 1])
        if d < 4:
            loop_send(r, d + 1)

    def down_copy(e, s, d, j):
        m = 17 if d == 4 else (d - 1) * 8 + j
        src = down_ref(e, -s * (d - 1), minor_off(j), d == 4)
        return rc(src, src, left.at[3], fr.at[e, m], at_z(s))

    def down_send(d, lo, hi):
        for j in range(lo, hi):
            for e, s in ways:
                down_copy(e, s, d, j).start()

    def down_got(d, j):
        m = 17 if d == 4 else (d - 1) * 8 + j
        for e, s in ways:
            got(down_ref(e, -s * d, minor_off(j), d == 4), fr.at[e, m])

    def chain(d):
        down_got(d, 0)
        if d < 4:
            down_send(d + 1, 0, 1)

    def pass_on(lo, hi):
        def one_row(j, _):
            down_got(1, j)
            for e, s in ways:
                down_copy(e, s, 2, j).start()
            return 0

        lax.fori_loop(lo, hi, one_row, 0)

    def take(lo, hi):
        def one_row(j, _):
            down_got(2, j)
            return 0

        lax.fori_loop(lo, hi, one_row, 0)

    class Exchange:
        def __init__(self, PB, RB, SND, RCV, ds, dr, ns, nr):
            self.PB, self.RB, self.SND, self.RCV = PB, RB, SND, RCV
            self.ds, self.dr, self.ns, self.nr = ds, dr, ns, nr

        def to_partner(self, k):
            for q in (2, 1, 3, 0):
                b = xm(q)
                put(self.PB.at[k, b * C + co], self.RB.at[k, b], self.ds, self.dr.at[k, q],
                    partner)

        def pair(self, k, q, side):
            b = xm(q)
            return self.PB[k, b * C + c, side].astype(F32) + self.RB[k, b, side].astype(F32)

        def partner_got(self, k, q):
            got(self.RB.at[k, xm(q)], self.dr.at[k, q])

        def send(self, k, slot, value, dirn):
            self.SND[k, slot] = value.astype(BF)
            put(self.SND.at[k, slot], self.RCV.at[k, slot], self.ns, self.nr.at[k, slot],
                at_x(dirn))

        def have(self, k, slot):
            got(self.RCV.at[k, slot], self.nr.at[k, slot])
            return self.RCV[k, slot].astype(F32)

        def far(self, k):
            self.partner_got(k, 2)
            self.send(k, 0, self.pair(k, 2, 0), 1)
            self.send(k, 1, self.pair(k, 2, 1), -1)
            self.partner_got(k, 1)
            self.send(k, 2, self.pair(k, 1, 1), 1)
            self.partner_got(k, 3)
            self.send(k, 3, self.pair(k, 3, 0), -1)

        def grow(self, k):
            self.send(k, 4, self.pair(k, 1, 0) + self.have(k, 0), 1)
            self.send(k, 5, self.pair(k, 3, 1) + self.have(k, 1), -1)

        def total(self, k):
            self.partner_got(k, 0)
            left = self.pair(k, 0, 0) + self.have(k, 3) + self.have(k, 4)
            right = self.pair(k, 0, 1) + self.have(k, 2) + self.have(k, 5)
            return left, right

    class Gather:
        def __init__(self, G, part, mine, s, r):
            self.G, self.part, self.mine, self.s, self.r = G, part, mine, s, r

        def ref(self, k, q, side, core):
            return self.G.at[(xm(q) * C + core, *self.part(k, side))]

        def go(self, k, slot, q, side, dev):
            ref = self.ref(k, q, side, c)
            src = self.mine.at[self.part(k, side)] if q == 0 else ref
            put(src, ref, self.s, self.r.at[k, slot], dev)

        def wait(self, k, slot, q, side, core):
            got(self.ref(k, q, side, core), self.r.at[k, slot])

        def own(self, k):
            self.go(k, 0, 0, 0, at_x(1))
            self.go(k, 1, 0, 1, at_x(-1))
            self.go(k, 2, 0, 1, at_x(1))
            self.go(k, 3, 0, 0, at_x(-1))
            self.go(k, 6, 0, 0, partner)
            self.go(k, 7, 0, 1, partner)

        def forward(self, k):
            self.wait(k, 0, 3, 0, c)
            self.go(k, 4, 3, 0, at_x(1))
            self.wait(k, 1, 1, 1, c)
            self.go(k, 5, 1, 1, at_x(-1))
            self.go(k, 8, 3, 0, partner)
            self.go(k, 9, 1, 1, partner)

        def forward2(self, k):
            self.wait(k, 2, 3, 1, c)
            self.go(k, 10, 3, 1, partner)
            self.wait(k, 3, 1, 0, c)
            self.go(k, 11, 1, 0, partner)

        def last(self, k):
            self.wait(k, 4, 2, 0, c)
            self.go(k, 12, 2, 0, partner)
            self.wait(k, 5, 2, 1, c)
            self.go(k, 13, 2, 1, partner)

        def finish(self, k):
            for slot, q, side in (
                (6, 0, 0), (7, 0, 1), (8, 3, 0), (9, 1, 1), (10, 3, 1), (11, 1, 0),
                (12, 2, 0), (13, 2, 1),
            ):
                self.wait(k, slot, q, side, co)

    one = Exchange(PB1, RB1, SND1, RCV1, left.at[4], d1r, left.at[5], n1r)
    two = Exchange(PB2, RB2, SND2, RCV2, left.at[6], d2r, left.at[7], n2r)
    rows = Gather(
        NALL, lambda k, side: (pl.ds(32 * k, 32), pl.ds(side * 1024, 1024)), NALL.at[x * C + c],
        left.at[8], a1r,
    )
    pairs = ((0, -1), (1, -3), (3, 4), (2, -2))

    def block_of(k, side):
        return (z + pairs[k][side] + 8) % 8

    def out_cols(k, side):
        return pl.ds(pl.multiple_of(block_of(k, side) * 256, 256), 256)

    done = Gather(out, lambda k, side: (slice(None), out_cols(k, side)), OWN, left.at[9], a2r)

    loads[0].wait()
    ring_send(0, 1)
    ring_send(1, 1)
    for copy in loads[1:4]:
        copy.wait()
    halo = []
    for i, ref in enumerate((KX, VX, DX)):
        part = [
            ref.at[pl.ds(n, 1)] if i == 2 else ref.at[:, pl.ds(128 * n, 128)] for n in range(6)
        ]
        put(part[4], part[0], left.at[10 + i], hr.at[0, i], after)
        put(part[1], part[5], left.at[10 + i], hr.at[1, i], before)
        halo.append((part[0], part[5]))

    row_send(0, 0)
    row_send(1, 0)

    def halo_got(side):
        for i in range(3):
            got(halo[i][side], hr.at[side, i])

    loads[4].wait()
    loop_send(0, 1)
    down_send(1, 0, 1)

    def head_norm(rows_, gain_, ones):
        wide = rows_.astype(F32)
        square = wide * wide
        high = square.astype(BF)
        low = (square - high.astype(F32)).astype(BF)
        mean = (
            jnp.dot(high, ones, preferred_element_type=F32)
            + jnp.dot(low, ones, preferred_element_type=F32)
        ) * (1.0 / 64)
        return (wide * lax.rsqrt(mean + EPS) * gain_).astype(BF)

    def iotas(rows_, cols_):
        return [lax.broadcasted_iota(jnp.int32, (rows_, cols_), i) for i in range(2)]

    r64, c64 = iotas(64, 64)
    kgain = jnp.sum(jnp.where(r64 == c64, kg[...], 0.0), axis=1, keepdims=True)
    r256, c256 = iotas(256, 256)
    ones256 = (r256 // 64 == c256 // 64).astype(BF)

    def key_norm(lo, n):
        wide = KX[:, lo:lo + n].astype(F32)
        mean = jnp.mean(wide * wide, axis=0, keepdims=True)
        KN[:, lo:lo + n] = (wide * lax.rsqrt(mean + EPS) * kgain).astype(BF)

    key_norm(128, 512)
    loads[5].wait()
    qgain = jnp.concatenate([qg[...]] * 4, axis=1)
    heads = [
        jnp.exp2(jnp.full((1, 1), (tp * 4 + h + 1).astype(F32) * -0.25)) for h in range(4)
    ]
    row = lax.broadcasted_iota(jnp.int32, (128, 128), 0)
    col = lax.broadcasted_iota(jnp.int32, (128, 128), 1)
    span = jnp.abs(
        lax.broadcasted_iota(jnp.int32, (128, 384), 1) - 128
        - lax.broadcasted_iota(jnp.int32, (128, 384), 0)
    ).astype(F32)

    def attend(b):
        qn = head_norm(QX[128 * b:128 * b + 128], qgain, ones256)
        kb, vb = KN[:, 128 * b:128 * b + 384], VX[:, 128 * b:128 * b + 384]
        docs = [DX[b + i].astype(F32) for i in range(3)]
        mine = jnp.transpose(jnp.broadcast_to(docs[1], (128, 128)))
        if b == 0:
            docs[0] = jnp.where(sp == 0, -1.0, docs[0])
        if b == 3:
            docs[2] = jnp.where(sp == Z * Y - 1, -1.0, docs[2])
        allowed = jnp.concatenate(
            [(mine == docs[0]) & (col >= row), mine == docs[1], (mine == docs[2]) & (col <= row)],
            axis=1,
        )
        outs = []
        for h in range(4):
            score = jnp.dot(qn[:, 64 * h:64 * h + 64], kb, preferred_element_type=F32)
            score = score * 0.125 - heads[h] * span
            score = jnp.where(allowed, score, -1e30)
            top = jnp.maximum(jnp.max(score, axis=1, keepdims=True), sink[h])
            p = jnp.exp(score - top)
            denom = jnp.sum(p, axis=1, keepdims=True) + jnp.exp(sink[h] - top)
            mixed = lax.dot_general(
                p.astype(BF), vb, (((1,), (1,)), ((), ())), preferred_element_type=F32
            )
            outs.append((mixed / denom).astype(BF))
        ATT[128 * b:128 * b + 128] = jnp.concatenate(outs, axis=1)

    def project(k):
        a = ATT[...].reshape(8, 2, 32, 256)[:, k].reshape(256, 256)
        p = jnp.dot(a, WO[...], preferred_element_type=F32).astype(BF)
        for side in range(2):
            PB1[k, :, side] = p[:, side * 1024:side * 1024 + 1024].reshape(8, 32, 1024)
        one.to_partner(k)

    def normalise(k):
        lo = 32 * k
        both = one.total(k)
        mid = (RES[lo:lo + 32].astype(F32) + jnp.concatenate(both, axis=1)).astype(BF).astype(F32)
        MID[lo:lo + 32] = mid
        scale = lax.rsqrt(jnp.mean(mid * mid, axis=-1, keepdims=True) + EPS)
        NALL[x * C + c, lo:lo + 32] = (mid * scale * gain[...]).astype(BF)
        rows.own(k)

    def up(n):
        lhs = NALL[...].reshape(512, 2048)
        rhs = WU[:, :, :, n * 512:n * 512 + 512].reshape(2048, 512)
        r = jnp.maximum(jnp.dot(lhs, rhs, preferred_element_type=F32), 0.0)
        ACT[:, n * 512:n * 512 + 512] = (r * r).astype(BF)

    def s_down(k):
        w = jnp.concatenate([WD[block_of(k, side)].reshape(256, 1024) for side in range(2)], axis=0)
        p = lax.dot_general(
            ACT[...], w, (((1,), (1,)), ((), ())), preferred_element_type=F32
        ).astype(BF)
        for side in range(2):
            PB2[k, :, side] = p[:, side * 256:side * 256 + 256].reshape(8, 64, 256)
        two.to_partner(k)

    def s_total(k):
        for side, part in enumerate(two.total(k)):
            cols = out_cols(k, side)
            OWN[:, cols] = (MID[:, cols] + part).astype(BF)
            keep.append(
                pltpu.make_async_copy(OWN.at[:, cols], out.at[x * C + c, :, cols], loc.at[8 + 2 * k + side])
            )
            keep[-1].start()
        done.own(k)

    keep = []
    def halo_block(side, lo, b):
        halo_got(side)
        key_norm(lo, 128)
        attend(b)

    for f, *args in (
        (attend, 1), (attend, 2), (ring_step, (0, 1), 1), (halo_block, 0, 0, 0),
        (halo_block, 1, 640, 3), (loads[6].wait,), (loads[7].wait,), (project, 0), (project, 1),
        (ring_step, (0, 1), 2), (pump, (0, 1), 0, 3), (one.far, 0), (chain, 1),
        (loop_step, 0, 1), (one.far, 1), (ring_step, (0, 1), 3), (pump, (0, 1), 3, 5),
        (pump, (0, 1), 8, 9), (one.grow, 0), (pump, (0, 1), 9, 11), (one.grow, 1),
        (ring_step, (0, 1), 4), (pump, (0, 1), 5, 7), (pump, (0, 1), 11, 12), (normalise, 0),
        (pump, (0, 1), 12, 13), (pump, (0, 1), 16, 17), (normalise, 1), (pump, (0, 1), 17, 18),
        (chain, 2), (loop_step, 0, 2), (pump, (0, 1), 18, 19), (pump, (0, 1), 7, 8),
        (rows.forward, 0), (pump, (0, 1), 13, 15), (rows.forward2, 0), (pump, (0, 1), 19, 21),
        (rows.forward, 1), (chain, 3), (loop_step, 0, 3), (rows.forward2, 1),
        (pump, (0, 1), 15, 16), (pump, (0, 1), 21, 22), (rows.last, 0), (pump, (0, 1), 22, 23),
        (pump, (0, 1), 24, 25), (loop_send, 1, 1), (down_send, 1, 1, 2), (rows.last, 1),
        (rows.finish, 0), (chain, 4), (loop_step, 0, 4), (pump, (0, 1), 23, 24),
        (loop_send, 2, 1), (loop_send, 3, 1), (down_send, 1, 2, 8), (rows.finish, 1),
        (pump, (0, 1), 25, 27), (loop_step, 1, 1), (pass_on, 1, 2), (pump, (0, 1), 27, 28),
        (up, 0), (up, 1), (loop_step, 2, 1), (pass_on, 2, 3), (loop_step, 3, 1), (pass_on, 3, 4),
        (loop_step, 1, 2), (pass_on, 4, 6), (loop_step, 2, 2), (pass_on, 6, 7),
        (loop_step, 3, 2), (pass_on, 7, 8), (s_down, 0), (loop_step, 1, 3), (take, 1, 2),
        (loop_step, 2, 3), (two.far, 0), (take, 2, 3), (loop_step, 3, 3), (loop_step, 1, 4),
        (s_down, 1), (loop_step, 2, 4), (take, 3, 4), (two.grow, 0), (loop_step, 3, 4),
        (s_down, 2), (two.far, 1), (take, 4, 6), (s_total, 0), (two.far, 2), (take, 6, 7),
        (two.grow, 1), (take, 7, 8), (s_down, 3), (done.forward, 0), (done.forward2, 0),
        (two.grow, 2), (two.far, 3), (s_total, 1), (done.last, 0), (s_total, 2),
        (done.finish, 0), (two.grow, 3), (done.forward, 1), (done.forward2, 1),
        (done.forward, 2), (done.forward2, 2), (s_total, 3), (done.last, 1), (done.last, 2),
        (done.finish, 1), (done.forward, 3), (done.finish, 2), (done.forward2, 3),
        (done.last, 3), (done.finish, 3),
    ):
        f(*args)
    for copy in keep:
        copy.wait()

    for i, ref in enumerate((
        WU.at[0, pl.ds(0, 7)], WU.at[pl.ds(0, 7)], WD.at[pl.ds(0, 7), pl.ds(0, 4)],
        WD.at[pl.ds(0, 7), pl.ds(0, 5)], RB1, SND1, RB2, SND2, NALL.at[pl.ds(0, 7)],
        NALL.at[pl.ds(0, 7)], KX.at[:, pl.ds(0, 256)], VX.at[:, pl.ds(0, 256)],
        DX.at[pl.ds(0, 2)],
    )):
        rc(ref, ref, left.at[i], hr.at[0, 0], partner).wait_send()


def shards(
    resid, queries, keys, values, documents, q_gain, k_gain, sink, w_out, n_gain, w_up, w_down
):
    rows, width = resid.shape
    vm, sm = pl.BlockSpec(memory_space=pltpu.VMEM), pl.BlockSpec(memory_space=pltpu.SMEM)
    hbm = pl.BlockSpec(memory_space=pltpu.HBM)
    H2 = 2048 // (2 * NC2)
    dma = pltpu.SemaphoreType.DMA
    out = pl.pallas_call(
        fused,
        out_shape=jax.ShapeDtypeStruct((8, rows // 8, width), BF),
        in_specs=[hbm, hbm, hbm, hbm, vm, vm, sm, hbm, hbm, vm, hbm, hbm],
        out_specs=pl.BlockSpec(memory_space=pl.ANY),
        scratch_shapes=[
            pltpu.VMEM((512, 256), BF),
            pltpu.VMEM((64, 768), BF),
            pltpu.VMEM((64, 768), BF),
            pltpu.VMEM((6, 1, 128), jnp.int32),
            pltpu.VMEM((64, 768), BF),
            pltpu.VMEM((512, 256), BF),
            pltpu.VMEM((8, 8, 32, 1024), BF),
            pltpu.VMEM((8, 8, 32, 1024), BF),
            pltpu.VMEM((256, 2048), BF),
            pltpu.VMEM((64, 2048), BF),
            pltpu.VMEM((NC1, 8, 2, 32, 1024), BF),
            pltpu.VMEM((NC1, 4, 2, 32, 1024), BF),
            pltpu.VMEM((NC1, 6, 32, 1024), BF),
            pltpu.VMEM((NC1, 6, 32, 1024), BF),
            pltpu.VMEM((NC2, 8, 2, 64, H2), BF),
            pltpu.VMEM((NC2, 4, 2, 64, H2), BF),
            pltpu.VMEM((NC2, 6, 64, H2), BF),
            pltpu.VMEM((NC2, 6, 64, H2), BF),
            pltpu.VMEM((8, 64, 2048), BF),
            pltpu.VMEM((64, 2048), F32),
            pltpu.VMEM((512, 1024), BF),
            pltpu.VMEM((64, 2048), BF),
            dma((16,)), dma((13,)), dma((2, 3)),
            dma((2, 2, 28)), dma((2, 2, 4)), dma((2, 18)), dma((4, 2, 4)),
            dma((NC1, 4)), dma((NC1, 6)), dma((NC2, 4)), dma((NC2, 6)),
            dma((NC1, 14)), dma((NC2, 14)),
        ],
        compiler_params=pltpu.CompilerParams(
            collective_id=0, has_side_effects=True, vmem_limit_bytes=56 * 1024 * 1024
        ),
        name="layer",
    )(
        queries, keys.T, values.T, documents.reshape(4, 1, 128), q_gain.reshape(1, -1),
        k_gain.reshape(1, -1), sink, w_out, resid, n_gain.reshape(1, -1), w_up, w_down.T,
    )
    return out.reshape(rows, width)


def solution(mesh):
    placed = (
        P("sp", None), P("sp", "tp"), P("sp", "tp"), P("sp", "tp"), P("sp"), P(), P(),
        P("tp"), P("tp", None), P(), P("sp", "tp"), P("tp", "sp"),
    )
    return jax.shard_map(
        shards, mesh=mesh, in_specs=placed, out_specs=P("sp", None), check_vma=False
    )
```

time: 103 us -> 98.3 us (0.954)
  Pallas kernels: 99.2 us -> 94.9 us
    pallas_call x1, Pallas kernels: 99.2 us -> 94.9 us  [shards(): pl.pallas_call(fused, out_shape=jax.ShapeDtypeStruct((8, rows // 8, width...]
where the time goes in v3:
time: 98.3 us; the launch traced here: 98.1 us
  Pallas kernels  94.9 us (97%)
  local copies, waits for them, and re-layouts  3.16 us (3%)
    pallas_call x1, Pallas kernels, shards(): pl.pallas_call(fused, out_shape=jax.ShapeDtypeStruct((8, rows // 8, width...  94.9 us
    unnamed x1, local copies, waits for them, and re-layouts  3.16 us

profile of v3, /device:TPU:1, one launch (start us, length us, event | category | flops | bytes accessed | tf_op | source)
XLA Modules:
  0.0 98.1 jit_solution(8621438427568771722)
XLA Ops:
  0.0 94.9 %layer.1 = bf16[8,64,2048]{2,1,0:T(8,128)(2,1)} custom-call(bf16[512,256]{1,0:T(8,128)(2,1)} %q_h.1, bf16[64,512]{1,0:T(8,128)(2,1)} %bitcast.9, bf16[64,512]{1,0:T(8,128)(2,1)} %bitcast.10, s32[4,1,128]{2,1,0:T(1,128)} %bitcast.13, f32[1,64]{1,0:T(1,128)} %bitcast.14, f32[1,64]{1,0:T(1,128)} %bitcast.15, f32[4]{0:T(128)} %sink.1, bf16[256,2048]{1,0:T(8,128)(2,1)} %wout_h.1, ...), custom_call_target="tpu_custom_call" | custom-call | tf_op jit(solution)/shard_map/layer/pallas_call | solution.py:502
  94.9 3.2 %copy.14 = bf16[512,2048]{1,0:T(8,128)(2,1)} copy(bf16[512,2048]{1,0:T(8,128)(2,1)} %bitcast.8) | data formatting | bytes 4194304

commit v4 on v3

--- a/solution.py
+++ b/solution.py
@@ -15,8 +15,8 @@
 
 
 def fused(
-    q_h, k_h, v_h, doc_h, qg, kg, sink, wout_h, resid_h, gain, wup_h, wdt_h, out,
-    QX, KX, VX, DX, KN, ATT, WU, WD, WO, RES, PB1, RB1, SND1, RCV1, PB2, RB2, SND2, RCV2, NALL, MID, ACT, OWN,
+    q_h, k_h, v_h, doc_h, qg_h, kg_h, sink_h, wout_h, resid_h, gain_h, wup_h, wdt_h, out,
+    qg, kg, sink, gain, QX, KX, VX, DX, KN, ATT, WU, WD, WO, RES, PB1, RB1, SND1, RCV1, PB2, RB2, SND2, RCV2, NALL, MID, ACT, OWN,
     loc, left, hr, gr, rr, fr, er, d1r, n1r, d2r, n2r, a1r, a2r,
 ):
     sp, tp = lax.axis_index("sp"), lax.axis_index("tp")
@@ -61,11 +61,15 @@
             resid_h.at[pl.ds(pl.multiple_of(tp * 64, 64), 64)], RES, loc.at[7]
         ),
     ]
-    for copy in loads:
+    small = [
+        pltpu.make_async_copy(src, dst, loc.at[16 + i])
+        for i, (src, dst) in enumerate(((qg_h, qg), (kg_h, kg), (sink_h, sink), (gain_h, gain)))
+    ]
+    for copy in loads[:5] + small + loads[5:]:
         copy.start()
     barrier = pltpu.get_barrier_semaphore()
     after, before = ((sp + 1) % (Z * Y), tp), ((sp + Z * Y - 1) % (Z * Y), tp)
-    near = [at_z(1), at_z(-1), at_y(1), at_y(-1), at_x(1), at_x(-1), partner, after, before]
+    near = [at_z(1), at_z(-1), at_y(1), at_y(-1), at_x(1), at_x(-1), at_x(2), partner, after, before]
     for dev in near:
         pl.semaphore_signal(barrier, inc=1, device_id=dev, device_id_type=MESH)
     pl.semaphore_wait(barrier, len(near))
@@ -85,7 +89,7 @@
         for e, s in ways:
             src = shard_ref(p, e, 0, -s * (d - 1), d == 4)
             dev = at_z(s) if pieces[p][3] == "z" else at_y(s)
-            put(src, src, left.at[0], rr.at[p, e, d - 1], dev)
+            put(src, src, left.at[0], rr.at[d - 1], dev)
 
     def minor_off(j):
         return jnp.where(j % 2 == 1, -((j + 1) // 2), j // 2)
@@ -93,60 +97,40 @@
     def row_copy(p, e, s, d, j, m):
         src = shard_ref(p, e, -s * (d - 1), minor_off(j), False)
         dev = at_y(s) if pieces[p][3] == "z" else at_z(s)
-        return rc(src, src, left.at[1], gr.at[p, e, m], dev)
-
-    def row_got(p, e, s, d, j, m):
-        got(shard_ref(p, e, -s * d, minor_off(j), False), gr.at[p, e, m])
+        return rc(src, src, left.at[1], gr.at[m], dev)
 
     def row_send(p, j):
         for e, s in ways:
             row_copy(p, e, s, 1, j, j).start()
 
-    def ring_step(ps, d):
-        for p in ps:
-            for e, s in ways:
-                got(shard_ref(p, e, 0, -s * d, d == 4), rr.at[p, e, d - 1])
-            if d < 4:
+    def ring_step(d):
+        got(WU.at[0, 0] if d == 4 else WU.at[0, pl.ds(0, 2)], rr.at[d - 1])
+        if d < 4:
+            for p in (0, 1):
                 ring_send(p, d + 1)
         for j in (2 * d - 1, 2 * d):
             if j < 8:
-                for p in ps:
+                for p in (0, 1):
                     row_send(p, j)
 
-    def pump(ps, lo, hi):
-        def on(m, _):
+    def pump(lo, hi):
+        def step(m, _, to):
             d, j = m // 8 + 1, m % 8
-            for p in ps:
+            got(WU.at[0, pl.ds(0, 2)], gr.at[m])
+            for p in (0, 1):
                 for e, s in ways:
-                    row_got(p, e, s, d, j, m)
-                    row_copy(p, e, s, d + 1, j, m + 8).start()
-            return 0
-
-        def half(m, _, to):
-            for p in ps:
-                for e, s in ways:
-                    row_got(p, e, s, 3, m - 16, m)
-                    if e == to:
+                    if to == (0, 1):
+                        row_copy(p, e, s, d + 1, j, m + 8).start()
+                    elif e in to:
                         row_copy(p, e, s, 4, m - 16, m + 8 - 4 * e).start()
             return 0
 
-        def last(m, _):
-            for p in ps:
-                for e, s in ways:
-                    row_got(p, e, s, 4, m - 24 + 4 * e, m)
-            return 0
-
-        for a, b, f in (
-            (0, 16, on),
-            (16, 20, functools.partial(half, to=0)),
-            (20, 24, functools.partial(half, to=1)),
-            (24, 28, last),
-        ):
+        for a, b, to in ((0, 16, (0, 1)), (16, 20, (0,)), (20, 24, (1,)), (24, 28, ())):
             a, b = max(a, lo), min(b, hi)
             if b - a == 1:
-                f(a, 0)
+                step(a, 0, to)
             elif a < b:
-                lax.fori_loop(a, b, f, 0)
+                lax.fori_loop(a, b, functools.partial(step, to=to), 0)
 
     ring_base = (0, -3, 3, 4)
 
@@ -157,18 +141,17 @@
     def loop_send(r, d):
         for e, s in ways:
             src = down_ref(e, ring_base[r], -s * (d - 1), d == 4)
-            put(src, src, left.at[2], er.at[r, e, d - 1], at_y(s))
+            put(src, src, left.at[2], er.at[r, d - 1], at_y(s))
 
     def loop_step(r, d):
-        for e, s in ways:
-            got(down_ref(e, ring_base[r], -s * d, d == 4), er.at[r, e, d - 1])
+        got(WD.at[0, 0] if d == 4 else WD.at[0, pl.ds(0, 2)], er.at[r, d - 1])
         if d < 4:
             loop_send(r, d + 1)
 
     def down_copy(e, s, d, j):
         m = 17 if d == 4 else (d - 1) * 8 + j
         src = down_ref(e, -s * (d - 1), minor_off(j), d == 4)
-        return rc(src, src, left.at[3], fr.at[e, m], at_z(s))
+        return rc(src, src, left.at[3], fr.at[m], at_z(s))
 
     def down_send(d, lo, hi):
         for j in range(lo, hi):
@@ -177,8 +160,7 @@
 
     def down_got(d, j):
         m = 17 if d == 4 else (d - 1) * 8 + j
-        for e, s in ways:
-            got(down_ref(e, -s * d, minor_off(j), d == 4), fr.at[e, m])
+        got(WD.at[0, 0] if d == 4 else WD.at[0, pl.ds(0, 2)], fr.at[m])
 
     def chain(d):
         down_got(d, 0)
@@ -230,12 +212,16 @@
 
         def far(self, k):
             self.partner_got(k, 2)
-            self.send(k, 0, self.pair(k, 2, 0), 1)
-            self.send(k, 1, self.pair(k, 2, 1), -1)
+            straight = self is two and k in direct
+            self.send(k, 0, self.pair(k, 2, 0), 2 if straight else 1)
+            self.send(k, 1, self.pair(k, 2, 1), 2 if straight else -1)
             self.partner_got(k, 1)
             self.send(k, 2, self.pair(k, 1, 1), 1)
             self.partner_got(k, 3)
             self.send(k, 3, self.pair(k, 3, 0), -1)
+            if straight:
+                self.send(k, 4, self.pair(k, 1, 0), 1)
+                self.send(k, 5, self.pair(k, 3, 1), -1)
 
         def grow(self, k):
             self.send(k, 4, self.pair(k, 1, 0) + self.have(k, 0), 1)
@@ -245,11 +231,14 @@
             self.partner_got(k, 0)
             left = self.pair(k, 0, 0) + self.have(k, 3) + self.have(k, 4)
             right = self.pair(k, 0, 1) + self.have(k, 2) + self.have(k, 5)
+            if self is two and k in direct:
+                left, right = left + self.have(k, 0), right + self.have(k, 1)
             return left, right
 
     class Gather:
-        def __init__(self, G, part, mine, s, r):
+        def __init__(self, G, part, mine, s, r, size, direct=()):
             self.G, self.part, self.mine, self.s, self.r = G, part, mine, s, r
+            self.size, self.direct = size, direct
 
         def ref(self, k, q, side, core):
             return self.G.at[(xm(q) * C + core, *self.part(k, side))]
@@ -257,7 +246,7 @@
         def go(self, k, slot, q, side, dev):
             ref = self.ref(k, q, side, c)
             src = self.mine.at[self.part(k, side)] if q == 0 else ref
-            put(src, ref, self.s, self.r.at[k, slot], dev)
+            put(src, ref, self.s, self.r.at[k, min(slot, 6)], dev)
 
         def wait(self, k, slot, q, side, core):
             got(self.ref(k, q, side, core), self.r.at[k, slot])
@@ -267,14 +256,19 @@
             self.go(k, 1, 0, 1, at_x(-1))
             self.go(k, 2, 0, 1, at_x(1))
             self.go(k, 3, 0, 0, at_x(-1))
+            if k in self.direct:
+                self.go(k, 4, 0, 0, at_x(2))
+                self.go(k, 5, 0, 1, at_x(2))
             self.go(k, 6, 0, 0, partner)
             self.go(k, 7, 0, 1, partner)
 
         def forward(self, k):
             self.wait(k, 0, 3, 0, c)
-            self.go(k, 4, 3, 0, at_x(1))
+            if k not in self.direct:
+                self.go(k, 4, 3, 0, at_x(1))
             self.wait(k, 1, 1, 1, c)
-            self.go(k, 5, 1, 1, at_x(-1))
+            if k not in self.direct:
+                self.go(k, 5, 1, 1, at_x(-1))
             self.go(k, 8, 3, 0, partner)
             self.go(k, 9, 1, 1, partner)
 
@@ -291,17 +285,13 @@
             self.go(k, 13, 2, 1, partner)
 
         def finish(self, k):
-            for slot, q, side in (
-                (6, 0, 0), (7, 0, 1), (8, 3, 0), (9, 1, 1), (10, 3, 1), (11, 1, 0),
-                (12, 2, 0), (13, 2, 1),
-            ):
-                self.wait(k, slot, q, side, co)
+            got(NALL.at[0] if self.size == 8 else NALL.at[pl.ds(0, 2)], self.r.at[k, 6])
 
     one = Exchange(PB1, RB1, SND1, RCV1, left.at[4], d1r, left.at[5], n1r)
     two = Exchange(PB2, RB2, SND2, RCV2, left.at[6], d2r, left.at[7], n2r)
     rows = Gather(
         NALL, lambda k, side: (pl.ds(32 * k, 32), pl.ds(side * 1024, 1024)), NALL.at[x * C + c],
-        left.at[8], a1r,
+        left.at[8], a1r, 16,
     )
     pairs = ((0, -1), (1, -3), (3, 4), (2, -2))
 
@@ -311,7 +301,8 @@
     def out_cols(k, side):
         return pl.ds(pl.multiple_of(block_of(k, side) * 256, 256), 256)
 
-    done = Gather(out, lambda k, side: (slice(None), out_cols(k, side)), OWN, left.at[9], a2r)
+    direct = ()
+    done = Gather(out, lambda k, side: (slice(None), out_cols(k, side)), OWN, left.at[9], a2r, 8, direct)
 
     loads[0].wait()
     ring_send(0, 1)
@@ -352,6 +343,8 @@
     def iotas(rows_, cols_):
         return [lax.broadcasted_iota(jnp.int32, (rows_, cols_), i) for i in range(2)]
 
+    for copy in small:
+        copy.wait()
     r64, c64 = iotas(64, 64)
     kgain = jnp.sum(jnp.where(r64 == c64, kg[...], 0.0), axis=1, keepdims=True)
     r256, c256 = iotas(256, 256)
@@ -450,33 +443,31 @@
         attend(b)
 
     for f, *args in (
-        (attend, 1), (attend, 2), (ring_step, (0, 1), 1), (halo_block, 0, 0, 0),
-        (halo_block, 1, 640, 3), (loads[6].wait,), (loads[7].wait,), (project, 0), (project, 1),
-        (ring_step, (0, 1), 2), (pump, (0, 1), 0, 3), (one.far, 0), (chain, 1),
-        (loop_step, 0, 1), (one.far, 1), (ring_step, (0, 1), 3), (pump, (0, 1), 3, 5),
-        (pump, (0, 1), 8, 9), (one.grow, 0), (pump, (0, 1), 9, 11), (one.grow, 1),
-        (ring_step, (0, 1), 4), (pump, (0, 1), 5, 7), (pump, (0, 1), 11, 12), (normalise, 0),
-        (pump, (0, 1), 12, 13), (pump, (0, 1), 16, 17), (normalise, 1), (pump, (0, 1), 17, 18),
-        (chain, 2), (loop_step, 0, 2), (pump, (0, 1), 18, 19), (pump, (0, 1), 7, 8),
-        (rows.forward, 0), (pump, (0, 1), 13, 15), (rows.forward2, 0), (pump, (0, 1), 19, 21),
-        (rows.forward, 1), (chain, 3), (loop_step, 0, 3), (rows.forward2, 1),
-        (pump, (0, 1), 15, 16), (pump, (0, 1), 21, 22), (rows.last, 0), (pump, (0, 1), 22, 23),
-        (pump, (0, 1), 24, 25), (loop_send, 1, 1), (down_send, 1, 1, 2), (rows.last, 1),
-        (rows.finish, 0), (chain, 4), (loop_step, 0, 4), (pump, (0, 1), 23, 24),
-        (loop_send, 2, 1), (loop_send, 3, 1), (down_send, 1, 2, 8), (rows.finish, 1),
-        (pump, (0, 1), 25, 27), (loop_step, 1, 1), (pass_on, 1, 2), (pump, (0, 1), 27, 28),
-        (up, 0), (up, 1), (loop_step, 2, 1), (pass_on, 2, 3), (loop_step, 3, 1), (pass_on, 3, 4),
-        (loop_step, 1, 2), (pass_on, 4, 6), (loop_step, 2, 2), (pass_on, 6, 7),
-        (loop_step, 3, 2), (pass_on, 7, 8), (s_down, 0), (loop_step, 1, 3), (take, 1, 2),
-        (loop_step, 2, 3), (two.far, 0), (take, 2, 3), (loop_step, 3, 3), (loop_step, 1, 4),
-        (s_down, 1), (loop_step, 2, 4), (take, 3, 4), (two.grow, 0), (loop_step, 3, 4),
-        (s_down, 2), (two.far, 1), (take, 4, 6), (s_total, 0), (two.far, 2), (take, 6, 7),
-        (two.grow, 1), (take, 7, 8), (s_down, 3), (done.forward, 0), (done.forward2, 0),
-        (two.grow, 2), (two.far, 3), (s_total, 1), (done.last, 0), (s_total, 2),
-        (done.finish, 0), (two.grow, 3), (done.forward, 1), (done.forward2, 1),
-        (done.forward, 2), (done.forward2, 2), (s_total, 3), (done.last, 1), (done.last, 2),
-        (done.finish, 1), (done.forward, 3), (done.finish, 2), (done.forward2, 3),
-        (done.last, 3), (done.finish, 3),
+        (attend, 1), (attend, 2), (ring_step, 1), (halo_block, 0, 0, 0), (pump, 0, 1),
+        (chain, 1), (halo_block, 1, 640, 3), (ring_step, 2), (loop_step, 0, 1), (loads[6].wait,),
+        (loads[7].wait,), (project, 0), (project, 1), (pump, 1, 3), (pump, 8, 9), (one.far, 0),
+        (one.far, 1), (chain, 2), (ring_step, 3), (pump, 3, 5), (loop_step, 0, 2), (one.grow, 0),
+        (pump, 9, 11), (pump, 16, 17), (chain, 3), (ring_step, 4), (one.grow, 1), (pump, 5, 7),
+        (pump, 11, 13), (normalise, 0), (loop_step, 0, 3), (normalise, 1), (pump, 17, 18),
+        (chain, 4), (pump, 18, 19), (down_send, 1, 1, 2), (pump, 7, 8), (pump, 13, 14),
+        (rows.forward, 0), (pump, 14, 15), (pump, 19, 20), (loop_send, 1, 1), (rows.forward2, 0),
+        (pump, 20, 21), (loop_step, 0, 4), (down_send, 1, 2, 3), (rows.forward, 1),
+        (pump, 15, 16), (pump, 21, 22), (rows.forward2, 1), (pump, 22, 23), (loop_send, 2, 1),
+        (rows.last, 0), (down_send, 1, 3, 4), (pump, 24, 25), (loop_send, 3, 1), (rows.last, 1),
+        (down_send, 1, 4, 5), (pump, 23, 24), (loop_step, 1, 1), (down_send, 1, 5, 8),
+        (pass_on, 1, 3), (pump, 25, 27), (loop_step, 2, 1), (pass_on, 3, 4), (loop_step, 3, 1),
+        (pass_on, 4, 5), (pump, 27, 28), (rows.finish, 0), (rows.finish, 1), (up, 0),
+        (loop_step, 1, 2), (up, 1), (loop_step, 2, 2), (pass_on, 5, 7), (loop_step, 3, 2),
+        (pass_on, 7, 8), (s_down, 0), (loop_step, 1, 3), (take, 1, 2), (two.far, 0),
+        (loop_step, 2, 3), (take, 2, 3), (loop_step, 3, 3), (take, 3, 4), (loop_step, 1, 4),
+        (s_down, 1), (two.grow, 0), (take, 4, 5), (loop_step, 2, 4), (two.far, 1), (take, 5, 6),
+        (loop_step, 3, 4), (s_down, 2), (take, 6, 7), (s_total, 0), (two.far, 2), (take, 7, 8),
+        (s_down, 3), (two.grow, 1), (two.far, 3), (done.forward, 0), (done.forward2, 0),
+        (two.grow, 2), (s_total, 1), (two.grow, 3), (done.last, 0), (s_total, 2),
+        (done.forward, 1), (done.forward2, 1), (s_total, 3), (done.forward, 2),
+        (done.forward2, 2), (done.last, 1), (done.forward, 3), (done.forward2, 3),
+        (done.last, 2), (done.last, 3), (done.finish, 0), (done.finish, 1), (done.finish, 2),
+        (done.finish, 3),
     ):
         f(*args)
     for copy in keep:
@@ -495,16 +486,19 @@
     resid, queries, keys, values, documents, q_gain, k_gain, sink, w_out, n_gain, w_up, w_down
 ):
     rows, width = resid.shape
-    vm, sm = pl.BlockSpec(memory_space=pltpu.VMEM), pl.BlockSpec(memory_space=pltpu.SMEM)
     hbm = pl.BlockSpec(memory_space=pltpu.HBM)
     H2 = 2048 // (2 * NC2)
     dma = pltpu.SemaphoreType.DMA
     out = pl.pallas_call(
         fused,
         out_shape=jax.ShapeDtypeStruct((8, rows // 8, width), BF),
-        in_specs=[hbm, hbm, hbm, hbm, vm, vm, sm, hbm, hbm, vm, hbm, hbm],
+        in_specs=[hbm] * 12,
         out_specs=pl.BlockSpec(memory_space=pl.ANY),
         scratch_shapes=[
+            pltpu.VMEM((1, 64), F32),
+            pltpu.VMEM((1, 64), F32),
+            pltpu.SMEM((4,), F32),
+            pltpu.VMEM((1, 2048), F32),
             pltpu.VMEM((512, 256), BF),
             pltpu.VMEM((64, 768), BF),
             pltpu.VMEM((64, 768), BF),
@@ -527,10 +521,10 @@
             pltpu.VMEM((64, 2048), F32),
             pltpu.VMEM((512, 1024), BF),
             pltpu.VMEM((64, 2048), BF),
-            dma((16,)), dma((13,)), dma((2, 3)),
-            dma((2, 2, 28)), dma((2, 2, 4)), dma((2, 18)), dma((4, 2, 4)),
+            dma((20,)), dma((13,)), dma((2, 3)),
+            dma((28,)), dma((4,)), dma((18,)), dma((4, 4)),
             dma((NC1, 4)), dma((NC1, 6)), dma((NC2, 4)), dma((NC2, 6)),
-            dma((NC1, 14)), dma((NC2, 14)),
+            dma((NC1, 7)), dma((NC2, 7)),
         ],
         compiler_params=pltpu.CompilerParams(
             collective_id=0, has_side_effects=True, vmem_limit_bytes=56 * 1024 * 1024

time: 98.3 us -> 91.1 us (0.927)
  Pallas kernels: 94.9 us -> 87.8 us
    pallas_call x1, Pallas kernels: 94.9 us -> 87.8 us  [shards(): pl.pallas_call(fused, out_shape=jax.ShapeDtypeStruct((8, rows // 8, width...]
where the time goes in v4:
time: 91.1 us; the launch traced here: 90.9 us
  Pallas kernels  87.8 us (96%)
  local copies, waits for them, and re-layouts  3.16 us (3%)
    pallas_call x1, Pallas kernels, shards(): pl.pallas_call(fused, out_shape=jax.ShapeDtypeStruct((8, rows // 8, width...  87.8 us
    unnamed x1, local copies, waits for them, and re-layouts  3.16 us

profile of v4, /device:TPU:1, one launch (start us, length us, event | category | flops | bytes accessed | tf_op | source)
XLA Modules:
  0.0 90.9 jit_solution(18358295833753174700)
XLA Ops:
  0.0 87.8 %layer.1 = bf16[8,64,2048]{2,1,0:T(8,128)(2,1)} custom-call(bf16[512,256]{1,0:T(8,128)(2,1)} %q_h.1, bf16[64,512]{1,0:T(8,128)(2,1)} %bitcast.9, bf16[64,512]{1,0:T(8,128)(2,1)} %bitcast.10, s32[4,1,128]{2,1,0:T(1,128)} %bitcast.13, f32[1,64]{1,0:T(1,128)} %bitcast.14, f32[1,64]{1,0:T(1,128)} %bitcast.15, f32[4]{0:T(128)} %sink_h.1, ...), custom_call_target="tpu_custom_call" | custom-call | tf_op jit(solution)/shard_map/layer/pallas_call | solution.py:492
  87.8 3.2 %copy.14 = bf16[512,2048]{1,0:T(8,128)(2,1)} copy(bf16[512,2048]{1,0:T(8,128)(2,1)} %bitcast.8) | data formatting | bytes 4194304

commit v5 on v4

--- a/solution.py
+++ b/solution.py
@@ -16,7 +16,7 @@
 
 def fused(
     q_h, k_h, v_h, doc_h, qg_h, kg_h, sink_h, wout_h, resid_h, gain_h, wup_h, wdt_h, out,
-    qg, kg, sink, gain, QX, KX, VX, DX, KN, ATT, WU, WD, WO, RES, PB1, RB1, SND1, RCV1, PB2, RB2, SND2, RCV2, NALL, MID, ACT, OWN,
+    qg, kg, sink, gain, QX, KX, VX, DX, KN, ATT, WU, WD, WO, RES, PB1, RB1, SND1, RCV1, PB2, RB2, SND2, RCV2, NALL, MID, ACT, ALL,
     loc, left, hr, gr, rr, fr, er, d1r, n1r, d2r, n2r, a1r, a2r,
 ):
     sp, tp = lax.axis_index("sp"), lax.axis_index("tp")
@@ -302,7 +302,10 @@
         return pl.ds(pl.multiple_of(block_of(k, side) * 256, 256), 256)
 
     direct = ()
-    done = Gather(out, lambda k, side: (slice(None), out_cols(k, side)), OWN, left.at[9], a2r, 8, direct)
+    done = Gather(
+        ALL, lambda k, side: (slice(None), out_cols(k, side)), ALL.at[x * C + c], left.at[9], a2r,
+        8, direct,
+    )
 
     loads[0].wait()
     ring_send(0, 1)
@@ -429,21 +432,29 @@
     def s_total(k):
         for side, part in enumerate(two.total(k)):
             cols = out_cols(k, side)
-            OWN[:, cols] = (MID[:, cols] + part).astype(BF)
+            ALL[x * C + c, :, cols] = (MID[:, cols] + part).astype(BF)
+        done.own(k)
+
+    keep = []
+
+    def hand_over(k):
+        done.finish(k)
+        for side in range(2):
+            cols = out_cols(k, side)
             keep.append(
-                pltpu.make_async_copy(OWN.at[:, cols], out.at[x * C + c, :, cols], loc.at[8 + 2 * k + side])
+                pltpu.make_async_copy(
+                    ALL.at[:, :, cols], out.at[:, :, cols], loc.at[8 + 2 * k + side]
+                )
             )
             keep[-1].start()
-        done.own(k)
-
-    keep = []
+
     def halo_block(side, lo, b):
         halo_got(side)
         key_norm(lo, 128)
         attend(b)
 
     for f, *args in (
-        (attend, 1), (attend, 2), (ring_step, 1), (halo_block, 0, 0, 0), (pump, 0, 1),
+        (attend, 1), (ring_step, 1), (attend, 2), (pump, 0, 1), (halo_block, 0, 0, 0),
         (chain, 1), (halo_block, 1, 640, 3), (ring_step, 2), (loop_step, 0, 1), (loads[6].wait,),
         (loads[7].wait,), (project, 0), (project, 1), (pump, 1, 3), (pump, 8, 9), (one.far, 0),
         (one.far, 1), (chain, 2), (ring_step, 3), (pump, 3, 5), (loop_step, 0, 2), (one.grow, 0),
@@ -466,8 +477,8 @@
         (two.grow, 2), (s_total, 1), (two.grow, 3), (done.last, 0), (s_total, 2),
         (done.forward, 1), (done.forward2, 1), (s_total, 3), (done.forward, 2),
         (done.forward2, 2), (done.last, 1), (done.forward, 3), (done.forward2, 3),
-        (done.last, 2), (done.last, 3), (done.finish, 0), (done.finish, 1), (done.finish, 2),
-        (done.finish, 3),
+        (hand_over, 0), (done.last, 2), (hand_over, 1), (done.last, 3), (hand_over, 2),
+        (hand_over, 3),
     ):
         f(*args)
     for copy in keep:
@@ -520,7 +531,7 @@
             pltpu.VMEM((8, 64, 2048), BF),
             pltpu.VMEM((64, 2048), F32),
             pltpu.VMEM((512, 1024), BF),
-            pltpu.VMEM((64, 2048), BF),
+            pltpu.VMEM((8, 64, 2048), BF),
             dma((20,)), dma((13,)), dma((2, 3)),
             dma((28,)), dma((4,)), dma((18,)), dma((4, 4)),
             dma((NC1, 4)), dma((NC1, 6)), dma((NC2, 4)), dma((NC2, 6)),

time: 91.1 us -> 90.3 us (level)
  no operation moved by 1% of the time
where the time goes in v5:
time: 90.3 us; the launch traced here: 90.2 us
  Pallas kernels  87 us (96%)
  local copies, waits for them, and re-layouts  3.16 us (3%)
    pallas_call x1, Pallas kernels, shards(): pl.pallas_call(fused, out_shape=jax.ShapeDtypeStruct((8, rows // 8, width...  87 us
    unnamed x1, local copies, waits for them, and re-layouts  3.16 us

profile of v5, /device:TPU:1, one launch (start us, length us, event | category | flops | bytes accessed | tf_op | source)
XLA Modules:
  0.0 90.2 jit_solution(17077096338144452098)
XLA Ops:
  0.0 87.0 %layer.1 = bf16[8,64,2048]{2,1,0:T(8,128)(2,1)} custom-call(bf16[512,256]{1,0:T(8,128)(2,1)} %q_h.1, bf16[64,512]{1,0:T(8,128)(2,1)} %bitcast.9, bf16[64,512]{1,0:T(8,128)(2,1)} %bitcast.10, s32[4,1,128]{2,1,0:T(1,128)} %bitcast.13, f32[1,64]{1,0:T(1,128)} %bitcast.14, f32[1,64]{1,0:T(1,128)} %bitcast.15, f32[4]{0:T(128)} %sink_h.1, ...), custom_call_target="tpu_custom_call" | custom-call | tf_op jit(solution)/shard_map/layer/pallas_call | solution.py:503
  87.0 3.2 %copy.14 = bf16[512,2048]{1,0:T(8,128)(2,1)} copy(bf16[512,2048]{1,0:T(8,128)(2,1)} %bitcast.8) | data formatting | bytes 4194304

commit v6 on v5

--- a/solution.py
+++ b/solution.py
@@ -455,8 +455,9 @@
 
     for f, *args in (
         (attend, 1), (ring_step, 1), (attend, 2), (pump, 0, 1), (halo_block, 0, 0, 0),
-        (chain, 1), (halo_block, 1, 640, 3), (ring_step, 2), (loop_step, 0, 1), (loads[6].wait,),
-        (loads[7].wait,), (project, 0), (project, 1), (pump, 1, 3), (pump, 8, 9), (one.far, 0),
+        (chain, 1), (ring_step, 2),
+        (halo_block, 1, 640, 3), (loop_step, 0, 1), (pump, 1, 3), (loads[6].wait,),
+        (loads[7].wait,), (project, 0), (pump, 8, 9), (project, 1), (one.far, 0),
         (one.far, 1), (chain, 2), (ring_step, 3), (pump, 3, 5), (loop_step, 0, 2), (one.grow, 0),
         (pump, 9, 11), (pump, 16, 17), (chain, 3), (ring_step, 4), (one.grow, 1), (pump, 5, 7),
         (pump, 11, 13), (normalise, 0), (loop_step, 0, 3), (normalise, 1), (pump, 17, 18),

time: 90.3 us -> 90 us (level)
  no operation moved by 1% of the time
where the time goes in v6:
time: 90 us; the launch traced here: 89.9 us
  Pallas kernels  86.7 us (96%)
  local copies, waits for them, and re-layouts  3.16 us (4%)
    pallas_call x1, Pallas kernels, shards(): pl.pallas_call(fused, out_shape=jax.ShapeDtypeStruct((8, rows // 8, width...  86.7 us
    unnamed x1, local copies, waits for them, and re-layouts  3.16 us

profile of v6, /device:TPU:1, one launch (start us, length us, event | category | flops | bytes accessed | tf_op | source)
XLA Modules:
  0.0 89.9 jit_solution(15762151025925385267)
XLA Ops:
  0.0 86.7 %layer.1 = bf16[8,64,2048]{2,1,0:T(8,128)(2,1)} custom-call(bf16[512,256]{1,0:T(8,128)(2,1)} %q_h.1, bf16[64,512]{1,0:T(8,128)(2,1)} %bitcast.9, bf16[64,512]{1,0:T(8,128)(2,1)} %bitcast.10, s32[4,1,128]{2,1,0:T(1,128)} %bitcast.13, f32[1,64]{1,0:T(1,128)} %bitcast.14, f32[1,64]{1,0:T(1,128)} %bitcast.15, f32[4]{0:T(128)} %sink_h.1, ...), custom_call_target="tpu_custom_call" | custom-call | tf_op jit(solution)/shard_map/layer/pallas_call | solution.py:504
  86.7 3.2 %copy.14 = bf16[512,2048]{1,0:T(8,128)(2,1)} copy(bf16[512,2048]{1,0:T(8,128)(2,1)} %bitcast.8) | data formatting | bytes 4194304
